TPU v7x, 256 devices: a whole 4x4x8 slice. The times are simulated.
256 devices in a mesh: ep: 64 (over z, y, core), tp: 4 (over x).
Axes of the slice: x: 4, y: 4, z: 8, core: 2. Of those that a mesh axis runs over, the one named last changes fastest.
Arguments:
- first_input: bfloat16 [32768, 2048], P('ep'), may hold values from -120 to 120
- first_gain: bfloat16 [2048], replicated, may hold values from 0.099609375 to 1.8984375
- pool_inward: bfloat16 [2048, 1024], P(None, 'tp'), may hold values from -0.125 to 0.125
- pool_mixing: bfloat16 [4, 256, 256], P('tp'), may hold values from -0.375 to 0.375
- pool_scale: bfloat16 [1024], P('tp'), may hold values from 0.099609375 to 1.8984375
- pool_outward: bfloat16 [1024, 2048], P('tp'), may hold values from -0.1875 to 0.1875
- second_input: bfloat16 [16384, 2048], P('ep'), may hold values from -120 to 120
- second_gain: bfloat16 [2048], replicated, may hold values from 0.099609375 to 1.8984375
- route_ids: int32 [16384, 2], P('ep'), may hold values from 0 to 31, all different within a row; in each aligned block of 256 rows (0 to 255, 256 to 511, ...) at most 18 rows name the same one
- route_logits: float32 [16384, 2], P('ep'), may hold values from -6 to 6
- expert_gate: bfloat16 [64, 2048, 2048], P('ep', None, 'tp'), may hold values from -0.125 to 0.125
- expert_up: bfloat16 [64, 2048, 2048], P('ep', None, 'tp'), may hold values from -0.125 to 0.125
- expert_down: bfloat16 [64, 2048, 2048], P('ep', 'tp'), may hold values from -0.09375 to 0.09375
Outputs:
- first_out: bfloat16 [32768, 2048], P('ep', 'tp')
- second_out: bfloat16 [16384, 2048], P('ep', 'tp')
Inputs may be any that keep to these rules, and one draw needn't show every extreme that they name: `route_ids`: each row names two different experts. In each aligned block of 256 rows (the rows of one index of ep) no expert is named by more than 18 rows, and in some blocks one expert is named by exactly 18 rows.
All inputs are finite; a program needn't handle non-finite values.
Results may differ from a plain program's by a relative error of at most 0.012.
Values may be sent and summed in bfloat16 or wider, within the bound.
A program may use at most 64 MiB of HBM per device.

v0:
```python
import jax
import jax.numpy as jnp
from jax import lax
from jax.sharding import PartitionSpec as P

epsilon = 1e-06


def from_behind(value, axis, steps):
    count = lax.axis_size(axis)
    leading, last = (max(0, -steps), min(count, count - steps))
    return lax.ppermute(value, axis, [(source, source + steps) for source in range(leading, last)])


def rms_scaled(values, weights):
    widened = values.astype(jnp.float32)
    inverse = lax.rsqrt(jnp.mean(widened * widened, axis=-1, keepdims=True) + epsilon)
    return (widened * inverse * weights.astype(jnp.float32)).astype(jnp.bfloat16)


def window_means(channels, length, offset):
    row_count = channels.shape[0] - 15
    summed = jnp.zeros((row_count, channels.shape[1]), jnp.float32)
    for lookback in range(16):
        summed = summed + jnp.where(
            lookback < length, channels[15 - lookback : 15 - lookback + row_count], 0.0
        )
    positions = offset + jnp.arange(row_count, dtype=jnp.int32)
    counts = jnp.minimum(positions + 1, length).astype(jnp.float32)
    return summed / counts[:, None]


def slot_positions(block_ids, expert_count, capacity):
    flattened = block_ids.reshape(-1)
    onehot = (flattened[:, None] == jnp.arange(expert_count, dtype=jnp.int32)[None, :]).astype(
        jnp.int32
    )
    running = jnp.cumsum(onehot, axis=0, dtype=jnp.int32) - 1
    slot_numbers = jnp.sum(onehot * running, axis=1)
    return flattened * capacity + slot_numbers


def expert_output(gate_sum, up_sum, down_rows):
    hidden = (jax.nn.silu(gate_sum) * up_sum).astype(jnp.bfloat16)
    return jnp.dot(hidden, down_rows, preferred_element_type=jnp.float32)


def local(
    first_input,
    first_gain,
    pool_inward,
    pool_mixing,
    pool_scale,
    pool_outward,
    second_input,
    second_gain,
    route_ids,
    route_logits,
    expert_gate,
    expert_up,
    expert_down,
):
    tensor_parts = lax.axis_size("tp")
    expert_count = lax.axis_size("ep") // 2
    model_width = first_input.shape[1]
    quarter_width = model_width // tensor_parts
    normed_first = rms_scaled(first_input, first_gain)
    pooled_in = jnp.dot(normed_first, pool_inward, preferred_element_type=jnp.float32).astype(
        jnp.bfloat16
    )
    halo_rows = from_behind(pooled_in[-15:], "ep", 1)
    extended = jnp.concatenate([halo_rows, pooled_in], axis=0).astype(jnp.float32)
    window = jnp.left_shift(jnp.int32(2), lax.axis_index("tp"))
    sequence_start = lax.axis_index("ep") * first_input.shape[0]
    means = window_means(extended, window, sequence_start)
    mixed = (means - pooled_in.astype(jnp.float32)).astype(jnp.bfloat16)
    pooled = (
        jnp.dot(mixed, pool_mixing[0], preferred_element_type=jnp.float32)
        * pool_scale.astype(jnp.float32)
    ).astype(jnp.bfloat16)
    mixer_term = jnp.dot(pooled, pool_outward, preferred_element_type=jnp.float32)
    normed_second = rms_scaled(second_input, second_gain)
    row_count = second_input.shape[0]
    capacity = 2 * row_count * 9 // (8 * expert_count)
    positions = slot_positions(route_ids, expert_count, capacity)
    repeated = jnp.repeat(normed_second, 2, axis=0)
    repeated = lax.dynamic_slice_in_dim(
        repeated, lax.axis_index("tp") * quarter_width, quarter_width, 1
    )
    send_width = repeated.shape[1]
    buffer = (
        jnp.zeros((expert_count * capacity, send_width), jnp.bfloat16).at[positions].set(repeated)
    )
    paired = jnp.broadcast_to(
        buffer.reshape(expert_count, 1, capacity, send_width),
        (expert_count, 2, capacity, send_width),
    ).reshape(2 * expert_count, capacity, send_width)
    arrived = lax.all_to_all(paired, "ep", split_axis=0, concat_axis=0, tiled=True)
    flattened = arrived.reshape(-1, quarter_width)
    portion = lax.all_gather(flattened, "tp", axis=1, tiled=True)
    gate_rows = expert_gate[0]
    up_rows = expert_up[0]
    gate_sum = jnp.dot(portion, gate_rows, preferred_element_type=jnp.float32)
    up_sum = jnp.dot(portion, up_rows, preferred_element_type=jnp.float32)
    flat_term = expert_output(gate_sum, up_sum, expert_down[0])
    first_summed, expert_summed = (
        lax.psum_scatter(
            mixer_term.astype(jnp.bfloat16), "tp", scatter_dimension=1, tiled=True
        ).astype(jnp.float32),
        lax.psum_scatter(
            flat_term.astype(jnp.bfloat16), "tp", scatter_dimension=1, tiled=True
        ).astype(jnp.float32),
    )
    first_out = first_summed.astype(jnp.bfloat16)
    half_out = expert_summed.astype(jnp.bfloat16).reshape(2 * expert_count, capacity, quarter_width)
    returned = lax.all_to_all(half_out, "ep", split_axis=0, concat_axis=0, tiled=True)
    route_out = jnp.sum(
        returned.reshape(expert_count, 2, capacity, quarter_width).astype(jnp.float32), axis=1
    ).reshape(-1, quarter_width)
    picked = route_out[positions].reshape(row_count, 2, quarter_width)
    shares = jax.nn.sigmoid(route_logits - route_logits[:, ::-1])
    second_out = jnp.sum(picked * shares[:, :, None], axis=1).astype(jnp.bfloat16)
    return (first_out, second_out)


def solution(mesh):
    placed = (
        P("ep", None),
        P(),
        P(None, "tp"),
        P("tp", None, None),
        P("tp"),
        P("tp", None),
        P("ep", None),
        P(),
        P("ep", None),
        P("ep", None),
        P("ep", None, "tp"),
        P("ep", None, "tp"),
        P("ep", "tp", None),
    )
    return jax.shard_map(
        local, mesh=mesh, in_specs=placed, out_specs=(P("ep", "tp"), P("ep", "tp")), check_vma=False
    )
```

profile of v0, /device:TPU:1, one launch (start us, length us, event | category | flops | bytes accessed | tf_op | source)
XLA Modules:
  0.0 273.8 jit_solution(5216356019160819248)
XLA Ops:
  7.2 1.0 copy.17
  8.5 0.7 broadcast_multiply_fusion
  9.2 1.2 reduce-window.6
  10.4 0.2 slice_reduce_fusion
  11.0 0.7 convert_element_type.83
  11.7 1.5 fusion.4
  13.2 0.3 fusion.6
  13.5 2.6 broadcast_in_dim.44
  16.1 4.1 %reshape.103 = bf16[512,2048]{1,0:T(8,128)(2,1)} reshape(bf16[256,2,2048]{2,1,0:T(2,128)(2,1)} %broadcast_in_dim.44) | data formatting | bytes 4194304 | tf_op jit(solution)/shard_map/reshape | solution.py:86
  20.4 3.0 %scatter_custom_fusion = bf16[576,512]{1,0:T(8,128)(2,1)S(1)} fusion(s32[512]{0:T(512)S(1)} %bitcast.41, bf16[512,2048]{1,0:T(8,128)(2,1)} %reshape.103, s32[]{:T(128)} %constant.31.clone.1, s32[]{:T(128)S(6)} %select_n.145, bf16[]{:T(256)} %constant.27.clone.1), kind=kCustom, calls=%fused_computation.61 | custom fusion | bytes 1115140 | tf_op jit(solution)/shard_map/scatter | solution.py:92
  23.4 0.2 broadcast_in_dim.45
  23.7 52.1 %all_to_all.10 = bf16[64,18,512]{2,1,0:T(8,128)(2,1)} all-to-all(bf16[64,18,512]{2,1,0:T(8,128)(2,1)S(1)} %bitcast.40), channel_id=1, replica_groups=mesh['ep'=64,'tp'=4] {'ep'}, dimensions={0} | all-to-all | bytes 2359296 | tf_op jit(solution)/shard_map/all_to_all | solution.py:98
  75.8 3.1 %reshape.105 = bf16[1152,512]{1,0:T(8,128)(2,1)} reshape(bf16[64,18,512]{2,1,0:T(8,128)(2,1)} %all_to_all.10) | data formatting | bytes 2359296 | tf_op jit(solution)/shard_map/reshape | solution.py:99
  78.9 0.2 reduce-scatter.5.cloned.1.call-start
  79.1 51.9 %all-gather.2.cloned.1.call-done = bf16[1152,2048]{1,0:T(8,128)(2,1)} async-done(((bf16[1152,512]{1,0:T(8,128)(2,1)}), bf16[1152,2048]{1,0:T(8,128)(2,1)}) %all-gather.2.cloned.1.call-update) | async-done | bytes 4718608 | tf_op jit(solution)/shard_map/all_gather | solution.py:100
  131.0 7.0 %fusion.11 = f32[1152,512]{1,0:T(8,128)} fusion(bf16[1152,2048]{1,0:T(8,128)(2,1)} %all-gather.2.cloned.1.call-done, bf16[1,2048,512]{2,1,0:T(8,128)(2,1)} %param.23), kind=kOutput, calls=%fused_computation.20 | convolution fusion | flops 2415919104 | bytes 9175040 | tf_op jit(solution)/shard_map/dot_general | solution.py:103
  138.0 11.0 %convolution_convert_fusion = bf16[1152,2048]{1,0:T(8,128)(2,1)} fusion(bf16[1,512,2048]{2,1,0:T(8,128)(2,1)S(1)} %copy-done, bf16[1152,2048]{1,0:T(8,128)(2,1)} %all-gather.2.cloned.1.call-done, f32[1152,512]{1,0:T(8,128)} %fusion.11, bf16[1,2048,512]{2,1,0:T(8,128)(2,1)} %param.24), kind=kOutput, calls=%fused_computation.2 | convolution fusion | flops 4837736448 | bytes 15990784 | tf_op jit(solution)/shard_map/dot_general | solution.py:45
  149.1 0.6 copy-done.4
  149.7 2.2 fusion
  152.0 2.0 fusion.15
  154.1 3.8 %collective-permute-start = (bf16[15,256]{1,0:T(8,128)(2,1)S(1)}, bf16[15,256]{1,0:T(8,128)(2,1)S(1)}, u32[]{:S(2)}, u32[]{:S(2)}) collective-permute-start(bf16[15,256]{1,0:T(8,128)(2,1)S(1)} %slice.78), channel_id=1, source_target_pairs={{0,4},{4,8},{8,12},{12,16},{16,20},{20,24},{24,28},{28,32},{32,36}... | collective-permute-start | bytes 23048 | tf_op jit(solution)/shard_map/ppermute | solution.py:12
  158.0 0.7 collective-permute-done
  158.7 4.7 %convolution_convert_fusion.1 = bf16[512,2048]{1,0:T(8,128)(2,1)} fusion(bf16[256,2048]{1,0:T(8,128)(2,1)} %param.18, f32[256]{0:T(256)S(1)} %convert_element_type.78, bf16[512,256]{1,0:T(8,128)(2,1)S(1)} %fusion.15, f32[527,256]{1,0:T(8,128)S(1)} %maximum_convert_fusion, f32[512]{0:T(512)S(1)} %minimum_convert_fusion, pred[]{:T(512)S(6)} %gt.63, ...), kind=kOutput, calls=%fused_computation.10 | convolution fusion | flops 609878016 | bytes 11930640 | tf_op jit(solution)/shard_map/dot_general | solution.py:81
  163.5 40.0 %reduce-scatter.5.cloned.1.call-done = bf16[1152,512]{1,0:T(8,128)(2,1)} async-done(((bf16[1152,2048]{1,0:T(8,128)(2,1)}), bf16[1152,512]{1,0:T(8,128)(2,1)}) %reduce-scatter.5.cloned.1.call-update) | async-done | bytes 1179664 | tf_op jit(solution)/shard_map/reduce_scatter | solution.py:110
  203.4 3.0 %reshape.106 = bf16[64,18,512]{2,1,0:T(8,128)(2,1)} reshape(bf16[1152,512]{1,0:T(8,128)(2,1)} %reduce-scatter.5.cloned.1.call-done) | data formatting | bytes 2359296 | tf_op jit(solution)/shard_map/reshape | solution.py:115
  206.5 11.1 %all-to-all-start.1 = ((bf16[64,18,512]{2,1,0:T(8,128)(2,1)}), bf16[64,18,512]{2,1,0:T(8,128)(2,1)}, u32[]{:S(2)}, u32[]{:S(2)}) async-start(bf16[64,18,512]{2,1,0:T(8,128)(2,1)} %reshape.106), calls=%async_computation.3 | async-start | bytes 3145728 | tf_op jit(solution)/shard_map/all_to_all | solution.py:116
  217.8 38.7 %all-to-all-done.1 = bf16[64,18,512]{2,1,0:T(8,128)(2,1)} async-done(((bf16[64,18,512]{2,1,0:T(8,128)(2,1)}), bf16[64,18,512]{2,1,0:T(8,128)(2,1)}, u32[]{:S(2)}, u32[]{:S(2)}) %all-to-all-start.1) | async-done | bytes 1179680 | tf_op jit(solution)/shard_map/all_to_all | solution.py:116
  256.5 3.0 %convert_reduce_fusion = f32[32,18,512]{2,1,0:T(8,128)} fusion(bf16[64,18,512]{2,1,0:T(8,128)(2,1)} %all-to-all-done.1), kind=kLoop, calls=%fused_computation.9 | loop fusion | flops 884736 | bytes 2359296 | tf_op jit(solution)/shard_map/reduce_sum | solution.py:117
  259.5 1.5 reshape.107
  261.1 2.3 gather_fusion
  263.4 1.8 reshape.108
  265.3 2.1 multiply_reduce_fusion
  (40 shorter events, 1.3 us)
Async XLA Ops:
  7.2 130.9 %copy-start = (bf16[1,512,2048]{2,1,0:T(8,128)(2,1)S(1)}, bf16[1,512,2048]{2,1,0:T(8,128)(2,1)}, u32[]{:S(2)}) copy-start(bf16[1,512,2048]{2,1,0:T(8,128)(2,1)} %param.25) | copy-start | bytes 6291460
  7.2 6.0 %copy-start.1 = (bf16[256,2048]{1,0:T(8,128)(2,1)S(1)}, bf16[256,2048]{1,0:T(8,128)(2,1)}, u32[]{:S(2)}) copy-start(bf16[256,2048]{1,0:T(8,128)(2,1)} %param.19) | copy-start | bytes 3145732
  7.2 123.8 %all-gather.2.cloned.1.call-start = ((), (), s32[]{:S(2)}) async-start(), calls=%async_computation.5 | async-start | bytes 5898240 | tf_op jit(solution)/shard_map/all_gather | solution.py:100
  78.9 124.5 %reduce-scatter.5.cloned.1.call-start = ((), (), s32[]{:S(2)}) async-start(), calls=%async_computation.6 | async-start | bytes 5898240 | tf_op jit(solution)/shard_map/reduce_scatter | solution.py:110
  149.0 0.7 copy-start.4
  149.1 118.2 %reduce-scatter.3.cloned.1.call-start = ((), (), s32[]{:S(2)}) async-start(), calls=%async_computation.4 | async-start | bytes 2621440 | tf_op jit(solution)/shard_map/reduce_scatter | solution.py:107
  149.7 2.2 copy-start.2
  152.0 6.0 %copy-start.6 = (bf16[256]{0:T(256)(128)(2,1)S(1)}, bf16[256]{0:T(256)(128)(2,1)}, u32[]{:S(2)}) copy-start(bf16[256]{0:T(256)(128)(2,1)} %param.17) | copy-start | bytes 1540
  152.0 6.7 %copy-start.5 = (bf16[1,256,256]{2,1,0:T(8,128)(2,1)S(1)}, bf16[1,256,256]{2,1,0:T(8,128)(2,1)}, u32[]{:S(2)}) copy-start(bf16[1,256,256]{2,1,0:T(8,128)(2,1)} %param.16) | copy-start | bytes 393220
  154.1 4.6 %collective-permute-start = (bf16[15,256]{1,0:T(8,128)(2,1)S(1)}, bf16[15,256]{1,0:T(8,128)(2,1)S(1)}, u32[]{:S(2)}, u32[]{:S(2)}) collective-permute-start(bf16[15,256]{1,0:T(8,128)(2,1)S(1)} %slice.78), channel_id=1, source_target_pairs={{0,4},{4,8},{8,12},{12,16},{16,20},{20,24},{24,28},{28,32},{32,36}... | collective-permute-start | bytes 23048 | tf_op jit(solution)/shard_map/ppermute | solution.py:12
  206.5 11.1 %copy-start.3 = (f32[256,2]{0,1:T(2,128)S(1)}, f32[256,2]{0,1:T(2,128)}, u32[]{:S(2)}) copy-start(f32[256,2]{0,1:T(2,128)} %param.22) | copy-start | bytes 6148
  206.5 50.1 %all-to-all-start.1 = ((bf16[64,18,512]{2,1,0:T(8,128)(2,1)}), bf16[64,18,512]{2,1,0:T(8,128)(2,1)}, u32[]{:S(2)}, u32[]{:S(2)}) async-start(bf16[64,18,512]{2,1,0:T(8,128)(2,1)} %reshape.106), calls=%async_computation.3 | async-start | bytes 3145728 | tf_op jit(solution)/shard_map/all_to_all | solution.py:116
Sparse Core Ops, SparseCore 0:
  79.0 51.9 all-gather.1
  149.2 54.1 reduce-scatter.4
  206.6 32.0 reduce-scatter.2
where the time goes:
time: 275 us; the launch traced here: 274 us
  waiting for transfers between devices  131 us (48%)
  blocking collectives  52.1 us (19%)
  matrix products  24.8 us (9%)
  local copies, waits for them, and re-layouts  24.5 us (9%)
  starting transfers between devices  15.2 us (6%)
  between operations  14 us (5%)
  other arithmetic  11.9 us (4%)
    all_to_all x1, blocking collectives, local(): lax.all_to_all(paired, 'ep', split_axis=0, concat_axis=0, tiled=True)  52.1 us
    all_gather x1, waiting for transfers between devices, local(): portion = lax.all_gather(flattened, 'tp', axis=1, tiled=True)  51.9 us
    reduce_scatter x1, waiting for transfers between devices, local(): lax.psum_scatter(flat_term.astype(jnp.bfloat16), 'tp', scatter_dimension=...  40 us
    all_to_all x1, waiting for transfers between devices, local(): lax.all_to_all(half_out, 'ep', split_axis=0, concat_axis=0, tiled=True)  38.7 us
    all_to_all x1, starting transfers between devices, local(): lax.all_to_all(half_out, 'ep', split_axis=0, concat_axis=0, tiled=True)  11.1 us
    dot_general x1, matrix products, expert_output(): return jnp.dot(hidden, down_rows, preferred_element_type=jnp.float32)  11 us
    dot_general x1, matrix products, local(): gate_sum = jnp.dot(portion, gate_rows, preferred_element_type=jnp.float32)  7.04 us
  transfers between devices with their start and end apart: 5, of which 4 were waited for; matrix products, arithmetic and copies ran while one was open for 8% of the time, Pallas kernels for 0%

commit v1 on v0

v1 whole, which is shorter than its diff:
```python
import jax
import jax.numpy as jnp
from jax import lax
from jax.experimental import pallas as pl
from jax.experimental.pallas import tpu as pltpu
from jax.sharding import PartitionSpec as P

MESH = pl.DeviceIdType.MESH
F32, BF16 = jnp.float32, jnp.bfloat16
EPS = 1e-06
ZN, YN, XN = 8, 4, 4
NB = ZN * YN
NG = ZN
EP = NB * 2
HALF = NB // 2


def dot(a, b):
    return jnp.dot(a, b, preferred_element_type=F32)


def dot_t(a, b):
    return lax.dot_general(a, b, (((0,), (0,)), ((), ())), preferred_element_type=F32)


def iota(shape, dim):
    return lax.broadcasted_iota(jnp.int32, shape, dim)


def group_dz(g):
    return jnp.where((g & 1) == 1, (g + 1) >> 1, (8 - (g >> 1)) & 7)


def kernel(
    x1_h, g1, pin_h, pmix, psc, pout_h, x2_h, g2, ids, lg, wg_h, wu_h, wd_h,
    out1, out2,
    x1, pin, x2, wg, wu, wd, wg2, wu2, wd2,
    n1, pl_in, ext, halo, tail, plx, wo, xq,
    s, r, lhs, hid, tm, rr, fin, ret, fm, fo,
    sem_in, ws_s, ws_r, a_s, a_r, g_s, g_r, t_s, t_r, b_s, b_r, h_s, h_r, wo_s, wo_r, wp_s, wp_r, p_s, p_r,
):
    ep, t = lax.axis_index("ep"), lax.axis_index("tp")
    c = lax.rem(ep, 2)
    chip = ep // 2
    y, z = lax.rem(chip, YN), chip // YN

    def at(dz, dy, dc=0):
        z2, y2, c2 = lax.rem(z + dz + ZN, ZN), lax.rem(y + dy + YN, YN), lax.rem(c + dc, 2)
        return ((z2 * YN + y2) * 2 + c2, t)

    def along(dx):
        return (ep, lax.rem(t + dx, XN))

    partner = at(0, 0, 1)
    following = (lax.rem(ep + 1, EP), t)
    previous = (lax.rem(ep + EP - 1, EP), t)

    def remote(src, dst, ss, rs, device):
        return pltpu.make_async_remote_copy(
            src_ref=src, dst_ref=dst, send_sem=ss, recv_sem=rs, device_id=device, device_id_type=MESH
        )

    loads = [
        pltpu.make_async_copy(a, b, sem_in.at[i])
        for i, (a, b) in enumerate(
            [(x2_h, x2), (x1_h, x1), (pin_h, pin), (wg_h.at[0], wg), (wu_h.at[0], wu), (wd_h.at[0], wd)]
        )
    ]
    for copy in loads:
        copy.start()

    bar = pltpu.get_barrier_semaphore()

    def greet(b, carry):
        pl.semaphore_signal(bar, inc=1, device_id=at(b // YN, lax.rem(b, YN)), device_id_type=MESH)
        return carry

    lax.fori_loop(1, NB, greet, 0)
    for dx in (1, 2, 3):
        pl.semaphore_signal(bar, inc=1, device_id=along(dx), device_id_type=MESH)
    pl.semaphore_signal(bar, inc=1, device_id=partner, device_id_type=MESH)
    pl.semaphore_signal(bar, inc=1, device_id=previous, device_id_type=MESH)

    expert = iota((256, NB), 1)
    one0 = (ids[:, 0:1] == expert).astype(F32)
    one1 = (ids[:, 1:2] == expert).astype(F32)
    lower = (iota((256, 256), 0) > iota((256, 256), 1)).astype(BF16)
    place = dot(lower, (one0 + one1).astype(BF16)) + 1.0

    def slot_maps(marks):
        held = (place * marks).astype(BF16)

        def spread(width, per):
            e, col = iota((NB, width), 0), iota((NB, width), 1) // per
            dz = group_dz(col // YN)
            hit = ((e // YN - z - dz + 2 * ZN) & (ZN - 1)) + ((lax.rem(e, YN) - y - lax.rem(col, YN) + 2 * YN) & (YN - 1))
            return dot(held, (hit == 0).astype(BF16))

        return spread(NB * 16, 16), spread(NB * 8, 8)

    slot_main = (lax.rem(iota((256, NB * 16), 1), 16) + 1).astype(F32)
    over_col = iota((256, NB * 8), 1)
    slot_over = (lax.rem(over_col // 4, 2) + 17).astype(F32)
    over_k = lax.rem(over_col, 4)

    loads[0].wait()

    def norm2(i, carry):
        rows = pl.ds(pl.multiple_of(i * 64, 64), 64)
        v = x2[rows, :].astype(F32)
        inv = lax.rsqrt(jnp.mean(v * v, axis=-1, keepdims=True) + EPS)
        cols = pl.ds(pl.multiple_of(t * 512, 512), 512)
        xq[rows, :] = (x2[rows, cols].astype(F32) * inv * g2[:, cols].astype(F32)).astype(BF16)
        return carry

    lax.fori_loop(0, 4, norm2, 0)
    in_main, in_over = slot_maps(one0 + one1)
    pick_main = (in_main == slot_main).astype(BF16)
    xv = xq[...]
    rows_main = dot_t(pick_main, xv)
    rows_over = jnp.zeros((NB * 8, 128), F32)
    for k in range(4):
        s[:, 16 * k : 16 * k + 16, :] = rows_main[:, 128 * k : 128 * k + 128].reshape(NB, 16, 128).astype(BF16)
        pick = jnp.logical_and(in_over == slot_over, over_k == k).astype(BF16)
        rows_over = rows_over + dot_t(pick, xv[:, 128 * k : 128 * k + 128])
    s[:, 64:72, :] = rows_over.reshape(NB, 8, 128).astype(BF16)
    r[0, 0] = s[0]

    pl.semaphore_wait(bar, NB - 1 + 3 + 2)

    def dispatch(b, carry):
        remote(
            s.at[b], r.at[0, b], a_s.at[b], a_r.at[b // YN], at(group_dz(b // YN), lax.rem(b, YN))
        ).start()
        return carry

    lax.fori_loop(1, NB, dispatch, 0)

    swaps = [
        remote(a, b, ws_s.at[i], ws_r.at[i], partner)
        for i, (a, b) in enumerate([(wg_h.at[0], wg2), (wu_h.at[0], wu2), (wd_h.at[0], wd2)])
    ]
    for copy in swaps:
        copy.start()

    half_rows = pl.ds(pl.multiple_of(c * 128, 128), 128)
    outward = []
    for dx in (1, 2, 3):
        cols = pl.ds(pl.multiple_of(lax.rem(t + dx, XN) * 512, 512), 512)
        outward.append(
            remote(pout_h.at[half_rows, cols], wo.at[dx, half_rows], wo_s.at[dx], wo_r.at[dx], along(dx))
        )
    for copy in outward:
        copy.start()
    own_out = pltpu.make_async_copy(
        pout_h.at[:, pl.ds(pl.multiple_of(t * 512, 512), 512)], wo.at[0], sem_in.at[6]
    )
    own_out.start()

    def gather(g):
        rows = pl.ds(pl.multiple_of(g * YN, YN), YN)
        return [remote(r.at[0, rows], r.at[dx, rows], g_s.at[dx, g], g_r.at[dx, g], along(dx)) for dx in (1, 3, 2)]

    def first_arrived():
        remote(s.at[pl.ds(1, 3)], r.at[0, pl.ds(1, 3)], a_s.at[0], a_r.at[0], partner).wait_recv()

    def arrived(g):
        rows = pl.ds(pl.multiple_of(g * YN, YN), YN)
        remote(s.at[rows], r.at[0, rows], a_s.at[0], a_r.at[g], partner).wait_recv()

    loads[1].wait()
    loads[2].wait()

    def norm1(i, carry):
        rows = pl.ds(pl.multiple_of(i * 64, 64), 64)
        v = x1[rows, :].astype(F32)
        inv = lax.rsqrt(jnp.mean(v * v, axis=-1, keepdims=True) + EPS)
        n1[rows, :] = (v * inv * g1[...].astype(F32)).astype(BF16)
        return carry

    lax.fori_loop(0, 8, norm1, 0)
    first_arrived()
    for copy in gather(0):
        copy.start()

    def inward(i, carry):
        rows = pl.ds(pl.multiple_of(i * 256, 256), 256)
        pl_in[rows, :] = dot(n1[rows, :], pin[...]).astype(BF16)
        return carry

    lax.fori_loop(0, 2, inward, 0)
    tail[...] = pl_in[496:512, :]
    halo_copy = remote(tail, halo, h_s, h_r, following)
    halo_copy.start()

    def pass_on(g, carry):
        arrived(g)
        for copy in gather(g):
            copy.start()
        return carry

    lax.fori_loop(1, 4, pass_on, 0)
    halo_copy.wait_recv()
    ext[0:16, :] = jnp.where(ep == 0, 0.0, halo[...].astype(F32))
    ext[16:528, :] = pl_in[...].astype(F32)
    window = jnp.left_shift(jnp.int32(2), t)
    reach = ext[...]
    total = jnp.zeros((528, 256), F32)
    for i in range(4):
        reach = reach + pltpu.roll(reach, 1 << i, 0)
        total = jnp.where(t == i, reach, total)
    count = jnp.minimum(ep * 512 + iota((512, 1), 0) + 1, window).astype(F32)
    mixed = (total[16:528, :] / count - ext[16:528, :]).astype(BF16)
    plx[0] = (dot(mixed, pmix[0]) * psc[...].astype(F32)).astype(BF16)
    for copy in outward:
        copy.wait_recv()
    shared = [
        remote(wo.at[dx, half_rows], wo.at[dx, half_rows], wp_s.at[dx], wp_r.at[dx], partner) for dx in (1, 2, 3)
    ]
    for copy in shared:
        copy.start()
    lax.fori_loop(4, NG, pass_on, 0)

    for copy in loads[3:]:
        copy.wait()
    for copy in swaps:
        copy.wait_recv()

    def expand(k):
        m, n = iota((HALF * 2, HALF * 8), 0), iota((HALF * 2, HALF * 8), 1)
        return (n == (m // 2) * 8 + lax.rem(m, 2) * 4 + k).astype(BF16)

    def collapse(k):
        n, m = iota((HALF * 8, HALF * 2), 0), iota((HALF * 8, HALF * 2), 1)
        return (n == (m // 2) * 8 + lax.rem(m, 2) * 4 + k).astype(BF16)

    def chunk(i, carry):
        blocks = pl.ds(pl.multiple_of(i * HALF, HALF), HALF)

        def take(j, carry2):
            for copy in gather(i * 4 + j):
                copy.wait_recv()
            return carry2

        lax.fori_loop(0, 4, take, 0)
        for dx in range(4):
            q = lax.rem(t - dx + XN, XN)
            over = r[dx, blocks, 64:72, :].astype(F32).reshape(HALF * 8, 128).astype(BF16)
            for k in range(4):
                cols = pl.ds(pl.multiple_of(q * 512 + 128 * k, 128), 128)
                lhs[0 : HALF * 16, cols] = r[dx, blocks, 16 * k : 16 * k + 16, :].reshape(HALF * 16, 128)
                lhs[HALF * 16 : HALF * 18, cols] = dot(expand(k), over).astype(BF16)

        def units(n, carry2):
            cols = pl.ds(pl.multiple_of(n * 256, 256), 256)
            for j, (a, b) in enumerate([(wg, wu), (wg2, wu2)]):
                gate, up = dot(lhs[...], a[:, cols]), dot(lhs[...], b[:, cols])
                hid[j, :, cols] = (gate / (1.0 + jnp.exp(-gate)) * up).astype(BF16)
            return carry2

        lax.fori_loop(0, 2, units, 0)
        for dx in (2, 1, 3, 0):
            q = lax.rem(t + dx, XN)
            over = jnp.zeros((HALF * 8, 128), F32)
            for n in range(2):
                cols = pl.ds(pl.multiple_of(q * 512 + 256 * n, 256), 256)
                term = dot(hid[0], wd[:, cols]) + dot(hid[1], wd2[:, cols])
                for m in range(2):
                    k = 2 * n + m
                    part = term[:, 128 * m : 128 * m + 128]
                    tm[dx, blocks, 16 * k : 16 * k + 16, :] = part[0 : HALF * 16].reshape(HALF, 16, 128).astype(BF16)
                    over = over + dot(collapse(k), part[HALF * 16 :].astype(BF16))
            tm[dx, blocks, 64:72, :] = over.reshape(HALF, 8, 128).astype(BF16)
            if dx:

                def give(j, carry2):
                    reduce_copy(i * 4 + j, dx).start()
                    return carry2

                lax.fori_loop(0, 4, give, 0)
        return carry

    def reduce_copy(g, dx):
        rows = pl.ds(pl.multiple_of(g * YN, YN), YN)
        return remote(tm.at[dx, rows], rr.at[dx, rows], t_s.at[dx, g], t_r.at[dx, g], along(dx))

    def back(b):
        return remote(
            fin.at[b], ret.at[b], b_s.at[b], b_r.at[b // YN], at(ZN - group_dz(b // YN), YN - lax.rem(b, YN))
        )

    def summed(g):
        rows = pl.ds(pl.multiple_of(g * YN, YN), YN)
        for dx in (1, 3, 2):
            reduce_copy(g, dx).wait_recv()
        v = tm[0, rows].astype(F32)
        for dx in (1, 2, 3):
            v = v + rr[dx, rows].astype(F32)
        fin[rows] = v.astype(BF16)

    def give_back(g, carry):
        summed(g)

        def one(dy, carry2):
            back(g * YN + dy).start()
            return carry2

        lax.fori_loop(0, YN, one, 0)
        return carry

    lax.fori_loop(0, 2, chunk, 0)

    spread_pooled = [remote(plx.at[0], plx.at[dx], p_s.at[dx], p_r.at[dx], along(dx)) for dx in (1, 3, 2)]
    for copy in spread_pooled:
        copy.start()

    summed(0)
    ret[0] = fin[0]

    def first_back(b, carry):
        back(b).start()
        return carry

    lax.fori_loop(1, YN, first_back, 0)
    lax.fori_loop(1, NG, give_back, 0)

    own_out.wait()
    for copy in shared:
        copy.wait_recv()
    for copy in spread_pooled:
        copy.wait_recv()
    for n in range(2):
        rows = slice(256 * n, 256 * n + 256)
        acc = dot(plx[0, rows, :], wo[0])
        for dx in (1, 2, 3):
            acc = acc + dot(plx[dx, rows, :], wo[dx])
        out1[rows, :] = acc.astype(BF16)

    logit0, logit1 = lg[:, 0:1], lg[:, 1:2]
    maps = [
        (slot_maps(one0), 1.0 / (1.0 + jnp.exp(logit1 - logit0))),
        (slot_maps(one1), 1.0 / (1.0 + jnp.exp(logit0 - logit1))),
    ]
    remote(fin.at[pl.ds(1, 3)], ret.at[pl.ds(1, 3)], b_s.at[0], b_r.at[0], partner).wait_recv()

    def returned(g, carry):
        rows = pl.ds(pl.multiple_of(g * YN, YN), YN)
        remote(fin.at[rows], ret.at[rows], b_s.at[0], b_r.at[g], partner).wait_recv()
        return carry

    lax.fori_loop(1, NG, returned, 0)
    for k in range(4):
        fm[:, 128 * k : 128 * k + 128] = ret[:, 16 * k : 16 * k + 16, :].reshape(NB * 16, 128)
    fo[...] = ret[:, 64:72, :].astype(F32).reshape(NB * 8, 128).astype(BF16)
    picks = []
    for (main, over), share in maps:
        base = dot((main == slot_main).astype(BF16), fm[...])
        picks.append((base, over == slot_over, share))
    for k in range(4):
        acc = jnp.zeros((256, 128), F32)
        for base, over, share in picks:
            extra = dot(jnp.logical_and(over, over_k == k).astype(BF16), fo[...])
            acc = acc + share * (base[:, 128 * k : 128 * k + 128] + extra)
        out2[:, 128 * k : 128 * k + 128] = acc.astype(BF16)

    def sent_blocks(b, carry):
        remote(s.at[b], r.at[0, b], a_s.at[b], a_r.at[0], partner).wait_send()
        back(b).wait_send()
        return carry

    lax.fori_loop(1, NB, sent_blocks, 0)

    def sent_groups(g, carry):
        for copy in gather(g):
            copy.wait_send()
        for dx in (1, 2, 3):
            reduce_copy(g, dx).wait_send()
        return carry

    lax.fori_loop(0, NG, sent_groups, 0)
    for copy in swaps + outward + shared + spread_pooled + [halo_copy]:
        copy.wait_send()


def local(
    first_input, first_gain, pool_inward, pool_mixing, pool_scale, pool_outward,
    second_input, second_gain, route_ids, route_logits, expert_gate, expert_up, expert_down,
):
    vmem = pl.BlockSpec(memory_space=pltpu.VMEM)
    far = pl.BlockSpec(memory_space=pl.ANY)
    dma = pltpu.SemaphoreType.DMA
    m = HALF * 18
    return pl.pallas_call(
        kernel,
        name="mixer_experts",
        out_shape=(jax.ShapeDtypeStruct((512, 512), BF16), jax.ShapeDtypeStruct((256, 512), BF16)),
        in_specs=[far, vmem, far, vmem, vmem, far, far, vmem, vmem, vmem, far, far, far],
        out_specs=(vmem, vmem),
        scratch_shapes=[
            pltpu.VMEM((512, 2048), BF16),
            pltpu.VMEM((2048, 256), BF16),
            pltpu.VMEM((256, 2048), BF16),
            pltpu.VMEM((2048, 512), BF16),
            pltpu.VMEM((2048, 512), BF16),
            pltpu.VMEM((512, 2048), BF16),
            pltpu.VMEM((2048, 512), BF16),
            pltpu.VMEM((2048, 512), BF16),
            pltpu.VMEM((512, 2048), BF16),
            pltpu.VMEM((512, 2048), BF16),
            pltpu.VMEM((512, 256), BF16),
            pltpu.VMEM((528, 256), F32),
            pltpu.VMEM((16, 256), BF16),
            pltpu.VMEM((16, 256), BF16),
            pltpu.VMEM((4, 512, 256), BF16),
            pltpu.VMEM((4, 256, 512), BF16),
            pltpu.VMEM((256, 512), BF16),
            pltpu.VMEM((NB, 72, 128), BF16),
            pltpu.VMEM((4, NB, 72, 128), BF16),
            pltpu.VMEM((m, 2048), BF16),
            pltpu.VMEM((2, m, 512), BF16),
            pltpu.VMEM((4, NB, 72, 128), BF16),
            pltpu.VMEM((4, NB, 72, 128), BF16),
            pltpu.VMEM((NB, 72, 128), BF16),
            pltpu.VMEM((NB, 72, 128), BF16),
            pltpu.VMEM((NB * 16, 512), BF16),
            pltpu.VMEM((NB * 8, 128), BF16),
            dma((7,)),
            dma((3,)), dma((3,)),
            dma((NB,)), dma((NG,)),
            dma((4, NG)), dma((4, NG)),
            dma((4, NG)), dma((4, NG)),
            dma((NB,)), dma((NG,)),
            dma, dma,
            dma((4,)), dma((4,)),
            dma((4,)), dma((4,)),
            dma((4,)), dma((4,)),
        ],
        compiler_params=pltpu.CompilerParams(
            collective_id=0, has_side_effects=True, vmem_limit_bytes=60 * 1024 * 1024
        ),
    )(
        first_input, first_gain.reshape(1, -1), pool_inward, pool_mixing, pool_scale.reshape(1, -1), pool_outward,
        second_input, second_gain.reshape(1, -1), route_ids, route_logits, expert_gate, expert_up, expert_down,
    )


def solution(mesh):
    placed = (
        P("ep", None), P(), P(None, "tp"), P("tp", None, None), P("tp"), P("tp", None),
        P("ep", None), P(), P("ep", None), P("ep", None),
        P("ep", None, "tp"), P("ep", None, "tp"), P("ep", "tp", None),
    )
    return jax.shard_map(
        local, mesh=mesh, in_specs=placed, out_specs=(P("ep", "tp"), P("ep", "tp")), check_vma=False
    )
```

time: 275 us -> 98.9 us (0.36)
  waiting for transfers between devices: 131 us -> 0 us
  Pallas kernels: 0 us -> 87.7 us
  blocking collectives: 52.1 us -> 0 us
  matrix products: 24.8 us -> 0 us
  starting transfers between devices: 15.2 us -> 0 us
  local copies, waits for them, and re-layouts: 24.5 us -> 10.3 us
  between operations: 14 us -> 0.64 us
  other arithmetic: 11.9 us -> 0 us
    pallas_call x0 -> x1, Pallas kernels: none -> 87.7 us  [local(): pl.pallas_call(kernel, name='mixer_experts', out_shape=(jax.ShapeDtypeStr...]
    all_to_all x1 -> x0, blocking collectives: 52.1 us -> none  [local(): lax.all_to_all(paired, 'ep', split_axis=0, concat_axis=0, tiled=True)]
    all_gather x1 -> x0, waiting for transfers between devices: 51.9 us -> none  [local(): portion = lax.all_gather(flattened, 'tp', axis=1, tiled=True)]
    reduce_scatter x2 -> x0, waiting for transfers between devices: 40 us -> none  [the longest x1 40 us: local(): lax.psum_scatter(flat_term.astype(jnp.bfloat16), 'tp', scatter_dimension=...]
    all_to_all x1 -> x0, waiting for transfers between devices: 38.7 us -> none  [local(): lax.all_to_all(half_out, 'ep', split_axis=0, concat_axis=0, tiled=True)]
    dot_general x4 -> x0, matrix products: 24.8 us -> none  [the longest x1 11 us: expert_output(): return jnp.dot(hidden, down_rows, preferred_element_type=jnp.float32)]
    all_to_all x1 -> x0, starting transfers between devices: 11.1 us -> none  [local(): lax.all_to_all(half_out, 'ep', split_axis=0, concat_axis=0, tiled=True)]
    reshape x5 -> x3, local copies, waits for them, and re-layouts: 13.6 us -> 3.81 us  [the longest x1 1.29 us: local(): second_gain.reshape(1, -1)]
  transfers between devices with their start and end apart: 5 -> 0, of which waited for: 4 -> 0; matrix products, arithmetic and copies ran while one was open for 8% -> 0% of each run, Pallas kernels for 0% -> 0%
where the time goes in v1:
time: 98.9 us; the launch traced here: 98.6 us
  Pallas kernels  87.7 us (89%)
  local copies, waits for them, and re-layouts  10.3 us (10%)
    pallas_call x1, Pallas kernels, local(): pl.pallas_call(kernel, name='mixer_experts', out_shape=(jax.ShapeDtypeStr...  87.7 us
    unnamed x4, local copies, waits for them, and re-layouts  6.49 us

profile of v1, /device:TPU:1, one launch (start us, length us, event | category | flops | bytes accessed | tf_op | source)
XLA Modules:
  0.0 98.6 jit_solution(2363754966668057514)
XLA Ops:
  0.6 1.2 %reshape.14.psc = bf16[1,256]{1,0:T(2,128)(2,1)} reshape(bf16[256]{0:T(256)(128)(2,1)} %param.17) | data formatting | bytes 1024 | tf_op jit(solution)/shard_map/reshape | solution.py:442
  1.9 1.3 %reshape.13.g1 = bf16[1,2048]{1,0:T(2,128)(2,1)} reshape(bf16[2048]{0:T(1024)(128)(2,1)} %param.14) | data formatting | bytes 8192 | tf_op jit(solution)/shard_map/reshape | solution.py:442
  3.1 1.3 %reshape.15.g2 = bf16[1,2048]{1,0:T(2,128)(2,1)} reshape(bf16[2048]{0:T(1024)(128)(2,1)} %param.20) | data formatting | bytes 8192 | tf_op jit(solution)/shard_map/reshape | solution.py:443
  4.4 1.5 %copy.15.ids = s32[256,2]{1,0:T(8,128)} copy(s32[256,2]{0,1:T(2,128)} %param.21) | data formatting | bytes 4096 | tf_op args[8]
  5.9 1.5 %copy.16.lg = f32[256,2]{1,0:T(8,128)} copy(f32[256,2]{0,1:T(2,128)} %param.22) | data formatting | bytes 4096 | tf_op args[9]
  7.4 87.7 %mixer_experts.1 = (bf16[512,512]{1,0:T(8,128)(2,1)}, bf16[256,512]{1,0:T(8,128)(2,1)}) custom-call(bf16[512,2048]{1,0:T(8,128)(2,1)} %x1_h.1, bf16[1,2048]{1,0:T(2,128)(2,1)} %reshape.13.g1, bf16[2048,256]{1,0:T(8,128)(2,1)} %pin_h.1, bf16[1,256,256]{2,1,0:T(8,128)(2,1)} %pmix.1, bf16[1,256]{1,0:T(2,128)(2,1)} %reshape.14.psc, bf16[256,2048]{1,0:T(8,128)(2,1)} %pout_h.1, ...), custom_call_target="tpu_custom_call" | custom-call | tf_op jit(solution)/shard_map/mixer_experts/pallas_call | solution.py:393
  95.0 1.9 %copy.19 = bf16[512,512]{1,0:T(8,128)(2,1)} copy(bf16[512,512]{1,0:T(8,128)(2,1)} %get-tuple-element.4) | data formatting | bytes 1048576
  96.9 1.7 %copy.20 = bf16[256,512]{1,0:T(8,128)(2,1)} copy(bf16[256,512]{1,0:T(8,128)(2,1)} %get-tuple-element.5) | data formatting | bytes 524288

commit v2 on v1

v2 whole, which is shorter than its diff:
```python
import jax
import jax.numpy as jnp
from jax import lax
from jax.experimental import pallas as pl
from jax.experimental.pallas import tpu as pltpu
from jax.sharding import PartitionSpec as P

MESH = pl.DeviceIdType.MESH
F32, BF16 = jnp.float32, jnp.bfloat16
EPS = 1e-06
ZN, YN, XN = 8, 4, 4
NB = ZN * YN
NG = ZN
EP = NB * 2
HALF = NB // 2
NR = 3
SELF = NB - YN


def dot(a, b):
    return jnp.dot(a, b, preferred_element_type=F32)


def dot_t(a, b):
    return lax.dot_general(a, b, (((0,), (0,)), ((), ())), preferred_element_type=F32)


def iota(shape, dim):
    return lax.broadcasted_iota(jnp.int32, shape, dim)


def group_dz(g):
    return jnp.where((g & 1) == 1, (7 - g) >> 1, 4 + (g >> 1))


def kernel(
    x1_h, g1, pin_h, pmix, psc, pout_h, x2_h, g2, ids, lg, wg_h, wu_h, wd_h,
    out1, out2,
    x1, pin, x2, wg, wu, wd, wg2, wu2, wd2,
    n1, pl_in, ext, halo, tail, plx, wo, xq,
    s, s2, r, lhs, hid, tm, rr, rv, fin, ret, fm, fo, o1, o2,
    sem_in, ws_s, ws_r, a_s, a_r, a2_s, a2_r, g_s, g_r, y_s, y_r, v_s, v_r, d_s, d_r,
    b_s, b_r, h_s, h_r, wo_s, wo_r, wy_s, wy_r, wp_s, wp_r, p_s, p_r, p2_s, p2_r,
):
    ep, t = lax.axis_index("ep"), lax.axis_index("tp")
    c = lax.rem(ep, 2)
    chip = ep // 2
    y, z = lax.rem(chip, YN), chip // YN

    def at(dz, dy, dc=0):
        z2, y2, c2 = lax.rem(z + dz + ZN, ZN), lax.rem(y + dy + YN, YN), lax.rem(c + dc, 2)
        return ((z2 * YN + y2) * 2 + c2, t)

    def along(dx):
        return (ep, lax.rem(t + dx, XN))

    def quarter(dx):
        return lax.rem(t + dx + XN, XN)

    partner = at(0, 0, 1)
    following = (lax.rem(ep + 1, EP), t)
    previous = (lax.rem(ep + EP - 1, EP), t)

    def remote(src, dst, ss, rs, device):
        return pltpu.make_async_remote_copy(
            src_ref=src, dst_ref=dst, send_sem=ss, recv_sem=rs, device_id=device, device_id_type=MESH
        )

    def blocks_of(g, first=0, count=YN):
        return pl.ds(g * YN + first, count)

    loads = [
        pltpu.make_async_copy(a, b, sem_in.at[i])
        for i, (a, b) in enumerate(
            [(x2_h, x2), (x1_h, x1), (pin_h, pin), (wg_h.at[0], wg), (wu_h.at[0], wu), (wd_h.at[0], wd)]
        )
    ]
    for copy in loads:
        copy.start()

    bar = pltpu.get_barrier_semaphore()

    def greet(b, carry):
        pl.semaphore_signal(bar, inc=1, device_id=at(group_dz(b // YN), lax.rem(b, YN)), device_id_type=MESH)
        return carry

    lax.fori_loop(0, SELF, greet, 0)
    lax.fori_loop(SELF + 1, NB, greet, 0)
    for dx in (1, 2, 3):
        pl.semaphore_signal(bar, inc=1, device_id=along(dx), device_id_type=MESH)
    pl.semaphore_signal(bar, inc=1, device_id=partner, device_id_type=MESH)
    pl.semaphore_signal(bar, inc=1, device_id=previous, device_id_type=MESH)

    expert = iota((NB, 256), 0)
    one0 = (ids[0:1, :] == expert).astype(F32)
    one1 = (ids[1:2, :] == expert).astype(F32)
    earlier = (iota((256, 256), 0) < iota((256, 256), 1)).astype(BF16)
    place = dot((one0 + one1).astype(BF16), earlier) + 1.0

    def slot_maps(marks):
        held = (place * marks).astype(BF16)

        def spread(width, per):
            e, col = iota((NB, width), 0), iota((NB, width), 1) // per
            dz = group_dz(col // YN)
            hit = ((e // YN - z - dz + 2 * ZN) & (ZN - 1)) + ((lax.rem(e, YN) - y - lax.rem(col, YN) + 2 * YN) & (YN - 1))
            return dot_t(held, (hit == 0).astype(BF16))

        return spread(NB * 16, 16), spread(NB * 8, 8)

    slot_main = (lax.rem(iota((256, NB * 16), 1), 16) + 1).astype(F32)
    over_col = iota((256, NB * 8), 1)
    slot_over = (lax.rem(over_col // 4, 2) + 17).astype(F32)
    over_k = lax.rem(over_col, 4)

    loads[0].wait()

    def norm2(i, carry):
        rows = pl.ds(pl.multiple_of(i * 64, 64), 64)
        v = x2[rows, :].astype(F32)
        inv = lax.rsqrt(jnp.mean(v * v, axis=-1, keepdims=True) + EPS)
        for j, dx in enumerate((0, 2)):
            cols = pl.ds(pl.multiple_of(quarter(dx) * 512, 512), 512)
            xq[j, rows, :] = (x2[rows, cols].astype(F32) * inv * g2[cols].astype(F32)).astype(BF16)
        return carry

    lax.fori_loop(0, 4, norm2, 0)
    in_main, in_over = slot_maps(one0 + one1)
    pick_main = (in_main == slot_main).astype(BF16)
    picks_over = [jnp.logical_and(in_over == slot_over, over_k == k).astype(BF16) for k in range(4)]
    for j, buf, skip in ((0, s, 0), (1, s2, NR * YN)):
        xv = xq[j]
        count = NB - skip
        rows_main = dot_t(pick_main[:, skip * 16 :], xv)
        rows_over = jnp.zeros((count * 8, 128), F32)
        for k in range(4):
            lanes = slice(128 * k, 128 * k + 128)
            buf[:, 16 * k : 16 * k + 16, :] = rows_main[:, lanes].reshape(count, 16, 128).astype(BF16)
            rows_over = rows_over + dot_t(picks_over[k][:, skip * 8 :], xv[:, lanes])
        buf[:, 64:72, :] = rows_over.reshape(count, 8, 128).astype(BF16)
        r[2 * j, SELF] = buf[SELF - skip]

    loads[1].wait()
    loads[2].wait()

    def normed1(rows):
        v = x1[rows, :].astype(F32)
        inv = lax.rsqrt(jnp.mean(v * v, axis=-1, keepdims=True) + EPS)
        return (v * inv * g1[...].astype(F32)).astype(BF16)

    tail[...] = dot(normed1(pl.ds(496, 16)), pin[...]).astype(BF16)
    halo_copy = remote(tail, halo, h_s, h_r, following)

    pl.semaphore_wait(bar, NB - 1 + 3 + 2)

    halo_copy.start()

    def toward(b):
        return at(group_dz(b // YN), lax.rem(b, YN))

    def dispatch(b, carry):
        remote(s.at[b], r.at[0, b], a_s, a_r.at[b // YN], toward(b)).start()
        return carry

    def dispatch2(b, carry):
        remote(s2.at[b - NR * YN], r.at[2, b], a2_s, a2_r.at[b // HALF], toward(b)).start()
        return carry

    lax.fori_loop(0, HALF, dispatch, 0)
    lax.fori_loop(NR * YN, HALF, dispatch2, 0)
    for send in (dispatch, dispatch2):
        lax.fori_loop(HALF, SELF, send, 0)
        lax.fori_loop(SELF + 1, NB, send, 0)

    swaps = [
        remote(a, b, ws_s.at[i], ws_r.at[i], partner)
        for i, (a, b) in enumerate([(wg_h.at[0], wg2), (wu_h.at[0], wu2), (wd_h.at[0], wd2)])
    ]
    for copy in swaps:
        copy.start()

    half_rows = pl.ds(pl.multiple_of(c * 128, 128), 128)
    piece = pl.ds(pl.multiple_of(c * 128 + y * 32, 32), 32)
    outward = []
    for dx in (1, 2, 3):
        cols = pl.ds(pl.multiple_of(quarter(dx) * 512, 512), 512)
        outward.append(remote(pout_h.at[piece, cols], wo.at[dx, piece], wo_s, wo_r, along(dx)))
    for copy in outward:
        copy.start()
    along_y = [
        remote(wo.at[pl.ds(1, 3), piece], wo.at[pl.ds(1, 3), piece], wy_s, wy_r, at(0, dy)) for dy in (1, 2, 3)
    ]
    shared = remote(wo.at[pl.ds(1, 3), half_rows], wo.at[pl.ds(1, 3), half_rows], wp_s, wp_r, partner)
    own_out = pltpu.make_async_copy(
        pout_h.at[:, pl.ds(pl.multiple_of(t * 512, 512), 512)], wo.at[0], sem_in.at[6]
    )
    own_out.start()

    def landed(ref, sem):
        remote(ref, ref, a_s, sem, partner).wait_recv()

    def left(ref, sem):
        remote(ref, ref, sem, a_r.at[0], partner).wait_send()

    def gather(g, dx):
        rows = blocks_of(g)
        arrival = g_r.at[dx // 2 * NR + g if g < NR else 2 * NR + g // 4]
        return remote(r.at[0, rows], r.at[dx, rows], g_s, arrival, along(dx))

    def relay(g, dx):
        rows = blocks_of(g, dx - 1, 2)
        return remote(r.at[dx, rows], r.at[2, rows], y_s, y_r, along(dx))

    def arrived(g):
        landed(s.at[pl.ds(0, 3 if g == NG - 1 else YN)], a_r.at[g])

    def pass_on(g):
        arrived(g)
        for dx in (1, 3):
            gather(g, dx).start()

    def relay_on(g):
        for dx in (1, 3):
            gather(g, dx).wait_recv()
            relay(g, dx).start()

    def norm1(i, carry):
        rows = pl.ds(pl.multiple_of(i * 64, 64), 64)
        n1[rows, :] = normed1(rows)
        return carry

    lax.fori_loop(0, 8, norm1, 0)
    def inward(i, carry):
        rows = pl.ds(pl.multiple_of(i * 256, 256), 256)
        pl_in[rows, :] = dot(n1[rows, :], pin[...]).astype(BF16)
        return carry

    lax.fori_loop(0, 2, inward, 0)

    halo_copy.wait_recv()
    ext[0:16, :] = jnp.where(ep == 0, 0.0, halo[...].astype(F32))
    ext[16:528, :] = pl_in[...].astype(F32)
    window = jnp.left_shift(jnp.int32(2), t)
    reach = ext[...]
    total = jnp.zeros((528, 256), F32)
    for i in range(4):
        reach = reach + pltpu.roll(reach, 1 << i, 0)
        total = jnp.where(t == i, reach, total)
    count = jnp.minimum(ep * 512 + iota((512, 1), 0) + 1, window).astype(F32)
    mixed = (total[16:528, :] / count - ext[16:528, :]).astype(BF16)
    plx[0] = (dot(mixed, pmix[0]) * psc[...].astype(F32)).astype(BF16)
    def pooled(dx):
        return remote(plx.at[0], plx.at[dx], p_s, p_r.at[dx // 2], along(dx))

    def pooled_on(dx):
        rows = pl.ds(128 * (dx - 1), 256)
        return remote(plx.at[dx, rows], plx.at[2, rows], p2_s, p2_r, along(dx))

    for dx in (1, 3):
        pooled(dx).start()

    pass_on(0)
    pass_on(1)
    relay_on(0)
    pass_on(2)
    relay_on(1)
    pass_on(3)
    relay_on(2)
    for dx in (1, 3):
        pooled(dx).wait_recv()
        pooled_on(dx).start()
    landed(wo.at[pl.ds(1, 3), piece], wo_r)
    for copy in along_y:
        copy.start()

    def expand(k):
        m, n = iota((HALF * 2, HALF * 8), 0), iota((HALF * 2, HALF * 8), 1)
        return (n == (m // 2) * 8 + lax.rem(m, 2) * 4 + k).astype(BF16)

    def collapse(k):
        n, m = iota((HALF * 8, HALF * 2), 0), iota((HALF * 8, HALF * 2), 1)
        return (n == (m // 2) * 8 + lax.rem(m, 2) * 4 + k).astype(BF16)

    def rows_in(i):
        blocks = pl.ds(i * HALF, HALF)
        for dx in range(4):
            q = quarter(-dx)
            over = r[dx, blocks, 64:72, :].astype(F32).reshape(HALF * 8, 128).astype(BF16)
            for k in range(4):
                cols = pl.ds(pl.multiple_of(q * 512 + 128 * k, 128), 128)
                lhs[0 : HALF * 16, cols] = r[dx, blocks, 16 * k : 16 * k + 16, :].reshape(HALF * 16, 128)
                lhs[HALF * 16 : HALF * 18, cols] = dot(expand(k), over).astype(BF16)

    def units(n, carry):
        cols = pl.ds(pl.multiple_of(n * 256, 256), 256)
        for j, (a, b) in enumerate([(wg, wu), (wg2, wu2)]):
            gate, up = dot(lhs[...], a[:, cols]), dot(lhs[...], b[:, cols])
            hid[j, :, cols] = (gate / (1.0 + jnp.exp(-gate)) * up).astype(BF16)
        return carry

    def down(i, dx):
        blocks = pl.ds(i * HALF, HALF)
        over = jnp.zeros((HALF * 8, 128), F32)
        for n in range(2):
            cols = pl.ds(pl.multiple_of(quarter(dx) * 512 + 256 * n, 256), 256)
            term = dot(hid[0], wd[:, cols]) + dot(hid[1], wd2[:, cols])
            for m in range(2):
                k = 2 * n + m
                part = term[:, 128 * m : 128 * m + 128]
                tm[dx, blocks, 16 * k : 16 * k + 16, :] = part[0 : HALF * 16].reshape(HALF, 16, 128).astype(BF16)
                over = over + dot(collapse(k), part[HALF * 16 :].astype(BF16))
        tm[dx, blocks, 64:72, :] = over.reshape(HALF, 8, 128).astype(BF16)

    def by_way(j, dx):
        rows = blocks_of(2 * j + dx // 2)
        return remote(tm.at[2, rows], rv.at[rows], v_s, v_r.at[dx // 2, j], along(dx))

    def direct(j, dx):
        g = 2 * j + 1 - dx // 2
        rows = blocks_of(g)
        return remote(tm.at[dx, rows], rr.at[dx // 2, rows], d_s, d_r.at[g], along(dx))

    def joined(j, dx):
        g = 2 * j + dx // 2
        rows = blocks_of(g)
        return remote(tm.at[dx, rows], rr.at[dx // 2, rows], d_s, d_r.at[g], along(dx))

    def each(first, last, action):
        def body(g, carry):
            action(g)
            return carry

        lax.fori_loop(first, last, body, 0)

    def start_by_way(j):
        for dx in (1, 3):
            by_way(j, dx).start()

    def join(j):
        for dx in (1, 3):
            by_way(j, dx).wait_recv()
            rows = blocks_of(2 * j + dx // 2)
            tm[dx, rows] = (tm[dx, rows].astype(F32) + rv[rows].astype(F32)).astype(BF16)
            joined(j, dx).start()

    def back(b):
        return remote(fin.at[b], ret.at[b], b_s, b_r, at(ZN - group_dz(b // YN), YN - lax.rem(b, YN)))

    def summed(g):
        rows = blocks_of(g)
        landed(s.at[pl.ds(0, 2 * YN)], d_r.at[g])
        v = tm[0, rows].astype(F32) + rr[0, rows].astype(F32) + rr[1, rows].astype(F32)
        fin[rows] = v.astype(BF16)

    def give_back(g):
        summed(g)
        for dy in range(YN):
            back(g * YN + dy).start()

    landed(s.at[pl.ds(0, NR * YN)], y_r)
    landed(s.at[pl.ds(0, 2 * YN)], g_r.at[2 * NR])
    landed(s.at[pl.ds(0, YN)], a2_r.at[0])
    for copy in loads[3:]:
        copy.wait()
    for copy in swaps:
        copy.wait_recv()
    pass_on(4)
    rows_in(0)
    pass_on(5)
    lax.fori_loop(0, 2, units, 0)
    pass_on(6)
    pass_on(7)
    down(0, 2)
    each(0, 2, start_by_way)
    for dx in (1, 3):
        down(0, dx)
        each(0, 2, lambda j: direct(j, dx).start())
    down(0, 0)
    landed(s, g_r.at[2 * NR + 1])
    landed(s.at[pl.ds(0, HALF - 1)], a2_r.at[1])
    rows_in(1)
    lax.fori_loop(0, 2, units, 0)
    landed(wo.at[pl.ds(1, 3), pl.ds(0, 96)], wy_r)
    shared.start()
    each(0, 2, join)

    down(1, 2)
    each(2, 4, start_by_way)
    for dx in (1, 3):
        down(1, dx)
        each(2, 4, lambda j: direct(j, dx).start())
    each(0, 4, give_back)
    down(1, 0)
    each(2, 4, join)
    each(4, NG - 1, give_back)
    summed(NG - 1)
    ret[SELF] = fin[SELF]
    for dy in range(1, YN):
        back(SELF + dy).start()

    row0 = iota((8, 256), 0) == 0
    gap = lg[1:2, :] - lg[0:1, :]
    shares = jnp.where(row0, 1.0 / (1.0 + jnp.exp(gap)), 1.0 / (1.0 + jnp.exp(-gap))).T
    maps = [(slot_maps(one0), shares[:, 0:1]), (slot_maps(one1), shares[:, 1:2])]
    own_out.wait()
    shared.wait_recv()
    landed(plx.at[0], p2_r)
    for n in range(2):
        rows = slice(256 * n, 256 * n + 256)
        acc = dot(plx[0, rows, :], wo[0])
        for dx in (1, 2, 3):
            acc = acc + dot(plx[dx, rows, :], wo[dx])
        o1[rows, :] = acc.astype(BF16)
    write1 = pltpu.make_async_copy(o1, out1, sem_in.at[7])
    write1.start()

    landed(s.at[pl.ds(0, NB - 1)], b_r)
    for k in range(4):
        fm[:, 128 * k : 128 * k + 128] = ret[:, 16 * k : 16 * k + 16, :].reshape(NB * 16, 128)
    fo[...] = ret[:, 64:72, :].astype(F32).reshape(NB * 8, 128).astype(BF16)
    picks = []
    for (main, over), share in maps:
        base = dot((main == slot_main).astype(BF16), fm[...])
        picks.append((base, over == slot_over, share))
    for k in range(4):
        acc = jnp.zeros((256, 128), F32)
        for base, over, share in picks:
            extra = dot(jnp.logical_and(over, over_k == k).astype(BF16), fo[...])
            acc = acc + share * (base[:, 128 * k : 128 * k + 128] + extra)
        o2[:, 128 * k : 128 * k + 128] = acc.astype(BF16)
    write2 = pltpu.make_async_copy(o2, out2, sem_in.at[8])
    write2.start()

    left(s.at[pl.ds(0, NB - 1)], a_s)
    left(s.at[pl.ds(0, NB - NR * YN - 1)], a2_s)
    left(r.at[pl.ds(0, 2)], g_s)
    left(s.at[pl.ds(0, NR * YN)], y_s)
    left(s, v_s)
    left(r.at[pl.ds(0, 2)], d_s)
    left(s.at[pl.ds(0, NB - 1)], b_s)
    left(plx.at[pl.ds(0, 2)], p_s)
    left(plx.at[0], p2_s)
    left(wo.at[pl.ds(1, 3), piece], wo_s)
    left(wo.at[pl.ds(1, 3), pl.ds(0, 96)], wy_s)
    for copy in swaps + [shared, halo_copy]:
        copy.wait_send()
    write1.wait()
    write2.wait()


def local(
    first_input, first_gain, pool_inward, pool_mixing, pool_scale, pool_outward,
    second_input, second_gain, route_ids, route_logits, expert_gate, expert_up, expert_down,
):
    vmem = pl.BlockSpec(memory_space=pltpu.VMEM)
    far = pl.BlockSpec(memory_space=pl.ANY)
    dma = pltpu.SemaphoreType.DMA
    m = HALF * 18
    return pl.pallas_call(
        kernel,
        name="mixer_experts",
        out_shape=(jax.ShapeDtypeStruct((512, 512), BF16), jax.ShapeDtypeStruct((256, 512), BF16)),
        in_specs=[far, vmem, far, vmem, vmem, far, far, vmem, vmem, vmem, far, far, far],
        out_specs=(far, far),
        scratch_shapes=[
            pltpu.VMEM((512, 2048), BF16),
            pltpu.VMEM((2048, 256), BF16),
            pltpu.VMEM((256, 2048), BF16),
            pltpu.VMEM((2048, 512), BF16),
            pltpu.VMEM((2048, 512), BF16),
            pltpu.VMEM((512, 2048), BF16),
            pltpu.VMEM((2048, 512), BF16),
            pltpu.VMEM((2048, 512), BF16),
            pltpu.VMEM((512, 2048), BF16),
            pltpu.VMEM((512, 2048), BF16),
            pltpu.VMEM((512, 256), BF16),
            pltpu.VMEM((528, 256), F32),
            pltpu.VMEM((16, 256), BF16),
            pltpu.VMEM((16, 256), BF16),
            pltpu.VMEM((4, 512, 256), BF16),
            pltpu.VMEM((4, 256, 512), BF16),
            pltpu.VMEM((2, 256, 512), BF16),
            pltpu.VMEM((NB, 72, 128), BF16),
            pltpu.VMEM((NB - NR * YN, 72, 128), BF16),
            pltpu.VMEM((4, NB, 72, 128), BF16),
            pltpu.VMEM((m, 2048), BF16),
            pltpu.VMEM((2, m, 512), BF16),
            pltpu.VMEM((4, NB, 72, 128), BF16),
            pltpu.VMEM((2, NB, 72, 128), BF16),
            pltpu.VMEM((NB, 72, 128), BF16),
            pltpu.VMEM((NB, 72, 128), BF16),
            pltpu.VMEM((NB, 72, 128), BF16),
            pltpu.VMEM((NB * 16, 512), BF16),
            pltpu.VMEM((NB * 8, 128), BF16),
            pltpu.VMEM((512, 512), BF16),
            pltpu.VMEM((256, 512), BF16),
            dma((9,)),
            dma((3,)), dma((3,)),
            dma, dma((NG,)),
            dma, dma((2,)),
            dma, dma((2 * NR + 2,)),
            dma, dma,
            dma, dma((2, 4)),
            dma, dma((NG,)),
            dma, dma,
            dma, dma,
            dma, dma,
            dma, dma,
            dma, dma,
            dma, dma((2,)),
            dma, dma,
        ],
        compiler_params=pltpu.CompilerParams(
            collective_id=0, has_side_effects=True, vmem_limit_bytes=60 * 1024 * 1024
        ),
    )(
        first_input, first_gain, pool_inward, pool_mixing, pool_scale, pool_outward,
        second_input, second_gain, route_ids.T, route_logits.T, expert_gate, expert_up, expert_down,
    )


def solution(mesh):
    placed = (
        P("ep", None), P(), P(None, "tp"), P("tp", None, None), P("tp"), P("tp", None),
        P("ep", None), P(), P("ep", None), P("ep", None),
        P("ep", None, "tp"), P("ep", None, "tp"), P("ep", "tp", None),
    )
    return jax.shard_map(
        local, mesh=mesh, in_specs=placed, out_specs=(P("ep", "tp"), P("ep", "tp")), check_vma=False
    )
```

time: 98.9 us -> 71.9 us (0.73)
  Pallas kernels: 87.7 us -> 66.9 us
  local copies, waits for them, and re-layouts: 10.3 us -> 3.54 us
    pallas_call x1, Pallas kernels: 87.7 us -> 66.9 us  [local(): pl.pallas_call(kernel, name='mixer_experts', out_shape=(jax.ShapeDtypeStr...]
    reshape x3 -> x0, local copies, waits for them, and re-layouts: 3.81 us -> none  [the longest x1 1.29 us: local(): second_gain.reshape(1, -1)]
    unnamed x4 -> x2, local copies, waits for them, and re-layouts: 6.49 us -> 3.54 us
where the time goes in v2:
time: 71.9 us; the launch traced here: 71.1 us
  Pallas kernels  66.9 us (93%)
  local copies, waits for them, and re-layouts  3.54 us (5%)
    pallas_call x1, Pallas kernels, local(): pl.pallas_call(kernel, name='mixer_experts', out_shape=(jax.ShapeDtypeStr...  66.9 us
    unnamed x2, local copies, waits for them, and re-layouts  3.54 us

profile of v2, /device:TPU:1, one launch (start us, length us, event | category | flops | bytes accessed | tf_op | source)
XLA Modules:
  0.0 71.1 jit_solution(6217756403864893464)
XLA Ops:
  0.6 66.9 %mixer_experts.1 = (bf16[512,512]{1,0:T(8,128)(2,1)}, bf16[256,512]{1,0:T(8,128)(2,1)}) custom-call(bf16[512,2048]{1,0:T(8,128)(2,1)} %x1_h.1, bf16[2048]{0:T(1024)(128)(2,1)} %g1.1, bf16[2048,256]{1,0:T(8,128)(2,1)} %pin_h.1, bf16[1,256,256]{2,1,0:T(8,128)(2,1)} %pmix.1, bf16[256]{0:T(256)(128)(2,1)} %psc.1, bf16[256,2048]{1,0:T(8,128)(2,1)} %pout_h.1, ...), custom_call_target="tpu_custom_call" | custom-call | tf_op jit(solution)/shard_map/mixer_experts/pallas_call | solution.py:459
  67.5 1.9 %copy.17 = bf16[512,512]{1,0:T(8,128)(2,1)} copy(bf16[512,512]{1,0:T(8,128)(2,1)} %get-tuple-element.4) | data formatting | bytes 1048576
  69.4 1.7 %copy.18 = bf16[256,512]{1,0:T(8,128)(2,1)} copy(bf16[256,512]{1,0:T(8,128)(2,1)} %get-tuple-element.5) | data formatting | bytes 524288

commit v3 on v2

--- a/solution.py
+++ b/solution.py
@@ -13,8 +13,9 @@
 NG = ZN
 EP = NB * 2
 HALF = NB // 2
+ORDER = (3, 5, 4, 0, 2, 6, 1, 7)
 NR = 3
-SELF = NB - YN
+SELF = 3 * YN
 
 
 def dot(a, b):
@@ -30,16 +31,19 @@
 
 
 def group_dz(g):
-    return jnp.where((g & 1) == 1, (7 - g) >> 1, 4 + (g >> 1))
+    dz = jnp.full_like(g, ORDER[0])
+    for i in range(1, NG):
+        dz = jnp.where(g == i, ORDER[i], dz)
+    return dz
 
 
 def kernel(
-    x1_h, g1, pin_h, pmix, psc, pout_h, x2_h, g2, ids, lg, wg_h, wu_h, wd_h,
+    x1_h, g1_h, pin_h, pmix_h, psc_h, pout_h, x2_h, g2_h, ids_h, lg_h, wg_h, wu_h, wd_h,
     out1, out2,
-    x1, pin, x2, wg, wu, wd, wg2, wu2, wd2,
+    ids, g2, g1, pmix, psc, lg, x1, pin, x2, wg, wu, wd, wg2, wu2,
     n1, pl_in, ext, halo, tail, plx, wo, xq,
-    s, s2, r, lhs, hid, tm, rr, rv, fin, ret, fm, fo, o1, o2,
-    sem_in, ws_s, ws_r, a_s, a_r, a2_s, a2_r, g_s, g_r, y_s, y_r, v_s, v_r, d_s, d_r,
+    s, s1, s2, s3, r, lhs, hid, tm, rr, rv, fin, ret, fm, fo,
+    sem_in, ws_s, ws_r, a_s, a_r, a2_s, n_s, n_r, g_s, g_r, y_s, y_r, v_s, v_r, d_s, d_r,
     b_s, b_r, h_s, h_r, wo_s, wo_r, wy_s, wy_r, wp_s, wp_r, p_s, p_r, p2_s, p2_r,
 ):
     ep, t = lax.axis_index("ep"), lax.axis_index("tp")
@@ -72,10 +76,14 @@
     loads = [
         pltpu.make_async_copy(a, b, sem_in.at[i])
         for i, (a, b) in enumerate(
-            [(x2_h, x2), (x1_h, x1), (pin_h, pin), (wg_h.at[0], wg), (wu_h.at[0], wu), (wd_h.at[0], wd)]
+            [(x2_h, x2), (x1_h, x1), (pin_h, pin), (wg_h.at[0], wg), (wu_h.at[0], wu), (wd_h.at[0], wd.at[pl.ds(0, 512)])]
         )
     ]
-    for copy in loads:
+    small = [
+        pltpu.make_async_copy(a, b, sem_in.at[7 + i])
+        for i, (a, b) in enumerate([(ids_h, ids), (g2_h, g2), (g1_h, g1), (pmix_h, pmix), (psc_h, psc), (lg_h, lg)])
+    ]
+    for copy in small + loads:
         copy.start()
 
     bar = pltpu.get_barrier_semaphore()
@@ -91,6 +99,8 @@
     pl.semaphore_signal(bar, inc=1, device_id=partner, device_id_type=MESH)
     pl.semaphore_signal(bar, inc=1, device_id=previous, device_id_type=MESH)
 
+    for copy in small:
+        copy.wait()
     expert = iota((NB, 256), 0)
     one0 = (ids[0:1, :] == expert).astype(F32)
     one1 = (ids[1:2, :] == expert).astype(F32)
@@ -119,17 +129,18 @@
         rows = pl.ds(pl.multiple_of(i * 64, 64), 64)
         v = x2[rows, :].astype(F32)
         inv = lax.rsqrt(jnp.mean(v * v, axis=-1, keepdims=True) + EPS)
-        for j, dx in enumerate((0, 2)):
-            cols = pl.ds(pl.multiple_of(quarter(dx) * 512, 512), 512)
-            xq[j, rows, :] = (x2[rows, cols].astype(F32) * inv * g2[cols].astype(F32)).astype(BF16)
+        for dx in range(4):
+            cols = pl.ds(pl.multiple_of(quarter(-dx) * 512, 512), 512)
+            xq[dx, rows, :] = (x2[rows, cols].astype(F32) * inv * g2[cols].astype(F32)).astype(BF16)
         return carry
 
     lax.fori_loop(0, 4, norm2, 0)
     in_main, in_over = slot_maps(one0 + one1)
     pick_main = (in_main == slot_main).astype(BF16)
     picks_over = [jnp.logical_and(in_over == slot_over, over_k == k).astype(BF16) for k in range(4)]
-    for j, buf, skip in ((0, s, 0), (1, s2, NR * YN)):
-        xv = xq[j]
+
+    def fill(buf, dx, skip):
+        xv = xq[dx]
         count = NB - skip
         rows_main = dot_t(pick_main[:, skip * 16 :], xv)
         rows_over = jnp.zeros((count * 8, 128), F32)
@@ -138,7 +149,9 @@
             buf[:, 16 * k : 16 * k + 16, :] = rows_main[:, lanes].reshape(count, 16, 128).astype(BF16)
             rows_over = rows_over + dot_t(picks_over[k][:, skip * 8 :], xv[:, lanes])
         buf[:, 64:72, :] = rows_over.reshape(count, 8, 128).astype(BF16)
-        r[2 * j, SELF] = buf[SELF - skip]
+        r[dx, SELF] = buf[SELF - skip]
+
+    fill(s, 0, 0)
 
     loads[1].wait()
     loads[2].wait()
@@ -158,26 +171,13 @@
     def toward(b):
         return at(group_dz(b // YN), lax.rem(b, YN))
 
-    def dispatch(b, carry):
-        remote(s.at[b], r.at[0, b], a_s, a_r.at[b // YN], toward(b)).start()
-        return carry
-
-    def dispatch2(b, carry):
-        remote(s2.at[b - NR * YN], r.at[2, b], a2_s, a2_r.at[b // HALF], toward(b)).start()
-        return carry
-
-    lax.fori_loop(0, HALF, dispatch, 0)
-    lax.fori_loop(NR * YN, HALF, dispatch2, 0)
-    for send in (dispatch, dispatch2):
-        lax.fori_loop(HALF, SELF, send, 0)
-        lax.fori_loop(SELF + 1, NB, send, 0)
-
-    swaps = [
-        remote(a, b, ws_s.at[i], ws_r.at[i], partner)
-        for i, (a, b) in enumerate([(wg_h.at[0], wg2), (wu_h.at[0], wu2), (wd_h.at[0], wd2)])
-    ]
-    for copy in swaps:
-        copy.start()
+    def send_blocks(buf, dx, skip, g, ss, arrival):
+        def body(dy, carry):
+            b = g * YN + dy
+            remote(buf.at[b - skip], r.at[dx, b], ss, arrival, at(ORDER[g], dy)).start()
+            return carry
+
+        lax.fori_loop(1 if ORDER[g] == 0 else 0, YN, body, 0)
 
     half_rows = pl.ds(pl.multiple_of(c * 128, 128), 128)
     piece = pl.ds(pl.multiple_of(c * 128 + y * 32, 32), 32)
@@ -191,6 +191,17 @@
         remote(wo.at[pl.ds(1, 3), piece], wo.at[pl.ds(1, 3), piece], wy_s, wy_r, at(0, dy)) for dy in (1, 2, 3)
     ]
     shared = remote(wo.at[pl.ds(1, 3), half_rows], wo.at[pl.ds(1, 3), half_rows], wp_s, wp_r, partner)
+    for g in range(NR):
+        send_blocks(s, 0, 0, g, a_s, a_r.at[g])
+    send_blocks(s, 0, 0, NR, a_s, n_r.at[0])
+
+    swaps = [
+        remote(a, b, ws_s.at[i], ws_r.at[i], partner)
+        for i, (a, b) in enumerate([(wg_h.at[0], wg2), (wu_h.at[0], wu2), (wd_h.at[0], wd.at[pl.ds(512, 512)])])
+    ]
+    for copy in swaps:
+        copy.start()
+
     own_out = pltpu.make_async_copy(
         pout_h.at[:, pl.ds(pl.multiple_of(t * 512, 512), 512)], wo.at[0], sem_in.at[6]
     )
@@ -204,7 +215,7 @@
 
     def gather(g, dx):
         rows = blocks_of(g)
-        arrival = g_r.at[dx // 2 * NR + g if g < NR else 2 * NR + g // 4]
+        arrival = g_r.at[2 * g + dx // 2 if g < NR - 1 else g // 4 + 2 * NR - 2]
         return remote(r.at[0, rows], r.at[dx, rows], g_s, arrival, along(dx))
 
     def relay(g, dx):
@@ -212,11 +223,11 @@
         return remote(r.at[dx, rows], r.at[2, rows], y_s, y_r, along(dx))
 
     def arrived(g):
-        landed(s.at[pl.ds(0, 3 if g == NG - 1 else YN)], a_r.at[g])
+        landed(s.at[pl.ds(0, YN)], a_r.at[g])
 
     def pass_on(g):
         arrived(g)
-        for dx in (1, 3):
+        for dx in (1, 3, 2) if g == NR - 1 else (1, 3):
             gather(g, dx).start()
 
     def relay_on(g):
@@ -259,26 +270,28 @@
     for dx in (1, 3):
         pooled(dx).start()
 
+    for dx in (1, 2, 3):
+        fill((s1, s2, s3)[dx - 1], dx, NR * YN)
+    for g in (3, 4, 5, 6, 7):
+        whole = ORDER[g] in (0, 1, 7)
+        for buf, dx, ss in ((s, 0, a_s), (s2, 2, a2_s), (s1, 1, n_s), (s3, 3, n_s)):
+            if dx == 0 and g > NR:
+                send_blocks(s, 0, 0, g, a_s, n_r.at[1] if whole else a_r.at[g])
+            elif dx == 2 or (dx and whole):
+                send_blocks(buf, dx, NR * YN, g, ss, n_r.at[g // 4])
     pass_on(0)
     pass_on(1)
+    pass_on(2)
     relay_on(0)
-    pass_on(2)
     relay_on(1)
-    pass_on(3)
-    relay_on(2)
-    for dx in (1, 3):
-        pooled(dx).wait_recv()
-        pooled_on(dx).start()
+    pass_on(4)
+    pass_on(5)
     landed(wo.at[pl.ds(1, 3), piece], wo_r)
     for copy in along_y:
         copy.start()
 
     def expand(k):
         m, n = iota((HALF * 2, HALF * 8), 0), iota((HALF * 2, HALF * 8), 1)
-        return (n == (m // 2) * 8 + lax.rem(m, 2) * 4 + k).astype(BF16)
-
-    def collapse(k):
-        n, m = iota((HALF * 8, HALF * 2), 0), iota((HALF * 8, HALF * 2), 1)
         return (n == (m // 2) * 8 + lax.rem(m, 2) * 4 + k).astype(BF16)
 
     def rows_in(i):
@@ -292,23 +305,25 @@
                 lhs[HALF * 16 : HALF * 18, cols] = dot(expand(k), over).astype(BF16)
 
     def units(n, carry):
-        cols = pl.ds(pl.multiple_of(n * 256, 256), 256)
+        cols = pl.ds(n * 256, 256) if isinstance(n, int) else pl.ds(pl.multiple_of(n * 256, 256), 256)
         for j, (a, b) in enumerate([(wg, wu), (wg2, wu2)]):
             gate, up = dot(lhs[...], a[:, cols]), dot(lhs[...], b[:, cols])
-            hid[j, :, cols] = (gate / (1.0 + jnp.exp(-gate)) * up).astype(BF16)
+            hid[:, pl.ds(512 * j + n * 256, 256) if isinstance(n, int) else pl.ds(pl.multiple_of(512 * j + n * 256, 256), 256)] = (gate / (1.0 + jnp.exp(-gate)) * up).astype(BF16)
         return carry
 
     def down(i, dx):
         blocks = pl.ds(i * HALF, HALF)
-        over = jnp.zeros((HALF * 8, 128), F32)
-        for n in range(2):
-            cols = pl.ds(pl.multiple_of(quarter(dx) * 512 + 256 * n, 256), 256)
-            term = dot(hid[0], wd[:, cols]) + dot(hid[1], wd2[:, cols])
-            for m in range(2):
-                k = 2 * n + m
-                part = term[:, 128 * m : 128 * m + 128]
-                tm[dx, blocks, 16 * k : 16 * k + 16, :] = part[0 : HALF * 16].reshape(HALF, 16, 128).astype(BF16)
-                over = over + dot(collapse(k), part[HALF * 16 :].astype(BF16))
+        cols = pl.ds(pl.multiple_of(quarter(dx) * 512, 512), 512)
+        term = dot(hid[...], wd[:, cols])
+        n, m = iota((HALF * 8, HALF * 2), 0), iota((HALF * 8, HALF * 2), 1)
+        spread = dot((n // 4 == m).astype(BF16), term[HALF * 16 :].astype(BF16))
+        lane_group = lax.rem(iota((HALF * 8, 128), 0), 4)
+        over = spread[:, 0:128]
+        for k in range(4):
+            part = term[0 : HALF * 16, 128 * k : 128 * k + 128]
+            tm[dx, blocks, 16 * k : 16 * k + 16, :] = part.reshape(HALF, 16, 128).astype(BF16)
+            if k:
+                over = jnp.where(lane_group == k, spread[:, 128 * k : 128 * k + 128], over)
         tm[dx, blocks, 64:72, :] = over.reshape(HALF, 8, 128).astype(BF16)
 
     def by_way(j, dx):
@@ -357,46 +372,46 @@
         for dy in range(YN):
             back(g * YN + dy).start()
 
-    landed(s.at[pl.ds(0, NR * YN)], y_r)
-    landed(s.at[pl.ds(0, 2 * YN)], g_r.at[2 * NR])
-    landed(s.at[pl.ds(0, YN)], a2_r.at[0])
+    landed(s.at[pl.ds(0, (NR - 1) * YN)], y_r)
+    landed(s.at[pl.ds(0, NR * YN)], g_r.at[2 * NR - 2])
+    landed(s.at[pl.ds(0, NR * YN)], n_r.at[0])
     for copy in loads[3:]:
         copy.wait()
     for copy in swaps:
         copy.wait_recv()
-    pass_on(4)
     rows_in(0)
-    pass_on(5)
     lax.fori_loop(0, 2, units, 0)
-    pass_on(6)
-    pass_on(7)
     down(0, 2)
     each(0, 2, start_by_way)
     for dx in (1, 3):
         down(0, dx)
         each(0, 2, lambda j: direct(j, dx).start())
     down(0, 0)
-    landed(s, g_r.at[2 * NR + 1])
-    landed(s.at[pl.ds(0, HALF - 1)], a2_r.at[1])
+    landed(s.at[pl.ds(0, HALF)], g_r.at[2 * NR - 1])
+    landed(r.at[pl.ds(0, 2), pl.ds(0, 20)], n_r.at[1])
     rows_in(1)
-    lax.fori_loop(0, 2, units, 0)
+    units(0, 0)
     landed(wo.at[pl.ds(1, 3), pl.ds(0, 96)], wy_r)
     shared.start()
     each(0, 2, join)
 
+    units(1, 0)
     down(1, 2)
     each(2, 4, start_by_way)
     for dx in (1, 3):
         down(1, dx)
         each(2, 4, lambda j: direct(j, dx).start())
-    each(0, 4, give_back)
     down(1, 0)
-    each(2, 4, join)
-    each(4, NG - 1, give_back)
-    summed(NG - 1)
+    each(0, NR, give_back)
+    summed(NR)
     ret[SELF] = fin[SELF]
     for dy in range(1, YN):
         back(SELF + dy).start()
+    each(2, 4, join)
+    for dx in (1, 3):
+        pooled(dx).wait_recv()
+        pooled_on(dx).start()
+    each(4, NG, give_back)
 
     row0 = iota((8, 256), 0) == 0
     gap = lg[1:2, :] - lg[0:1, :]
@@ -410,9 +425,7 @@
         acc = dot(plx[0, rows, :], wo[0])
         for dx in (1, 2, 3):
             acc = acc + dot(plx[dx, rows, :], wo[dx])
-        o1[rows, :] = acc.astype(BF16)
-    write1 = pltpu.make_async_copy(o1, out1, sem_in.at[7])
-    write1.start()
+        out1[rows, :] = acc.astype(BF16)
 
     landed(s.at[pl.ds(0, NB - 1)], b_r)
     for k in range(4):
@@ -427,14 +440,13 @@
         for base, over, share in picks:
             extra = dot(jnp.logical_and(over, over_k == k).astype(BF16), fo[...])
             acc = acc + share * (base[:, 128 * k : 128 * k + 128] + extra)
-        o2[:, 128 * k : 128 * k + 128] = acc.astype(BF16)
-    write2 = pltpu.make_async_copy(o2, out2, sem_in.at[8])
-    write2.start()
+        out2[:, 128 * k : 128 * k + 128] = acc.astype(BF16)
 
     left(s.at[pl.ds(0, NB - 1)], a_s)
     left(s.at[pl.ds(0, NB - NR * YN - 1)], a2_s)
-    left(r.at[pl.ds(0, 2)], g_s)
-    left(s.at[pl.ds(0, NR * YN)], y_s)
+    left(s.at[pl.ds(0, 22)], n_s)
+    left(r.at[pl.ds(0, 2), pl.ds(0, 22)], g_s)
+    left(s.at[pl.ds(0, (NR - 1) * YN)], y_s)
     left(s, v_s)
     left(r.at[pl.ds(0, 2)], d_s)
     left(s.at[pl.ds(0, NB - 1)], b_s)
@@ -444,8 +456,6 @@
     left(wo.at[pl.ds(1, 3), pl.ds(0, 96)], wy_s)
     for copy in swaps + [shared, halo_copy]:
         copy.wait_send()
-    write1.wait()
-    write2.wait()
 
 
 def local(
@@ -459,19 +469,24 @@
     return pl.pallas_call(
         kernel,
         name="mixer_experts",
-        out_shape=(jax.ShapeDtypeStruct((512, 512), BF16), jax.ShapeDtypeStruct((256, 512), BF16)),
-        in_specs=[far, vmem, far, vmem, vmem, far, far, vmem, vmem, vmem, far, far, far],
-        out_specs=(far, far),
+        out_shape=(pltpu.VMEM((512, 512), BF16), pltpu.VMEM((256, 512), BF16)),
+        in_specs=[far] * 13,
+        out_specs=(vmem, vmem),
         scratch_shapes=[
+            pltpu.VMEM((2, 256), jnp.int32),
+            pltpu.VMEM((2048,), BF16),
+            pltpu.VMEM((2048,), BF16),
+            pltpu.VMEM((1, 256, 256), BF16),
+            pltpu.VMEM((256,), BF16),
+            pltpu.VMEM((2, 256), F32),
             pltpu.VMEM((512, 2048), BF16),
             pltpu.VMEM((2048, 256), BF16),
             pltpu.VMEM((256, 2048), BF16),
             pltpu.VMEM((2048, 512), BF16),
             pltpu.VMEM((2048, 512), BF16),
-            pltpu.VMEM((512, 2048), BF16),
+            pltpu.VMEM((1024, 2048), BF16),
             pltpu.VMEM((2048, 512), BF16),
             pltpu.VMEM((2048, 512), BF16),
-            pltpu.VMEM((512, 2048), BF16),
             pltpu.VMEM((512, 2048), BF16),
             pltpu.VMEM((512, 256), BF16),
             pltpu.VMEM((528, 256), F32),
@@ -479,12 +494,14 @@
             pltpu.VMEM((16, 256), BF16),
             pltpu.VMEM((4, 512, 256), BF16),
             pltpu.VMEM((4, 256, 512), BF16),
-            pltpu.VMEM((2, 256, 512), BF16),
+            pltpu.VMEM((4, 256, 512), BF16),
             pltpu.VMEM((NB, 72, 128), BF16),
+            pltpu.VMEM((NB - NR * YN, 72, 128), BF16),
+            pltpu.VMEM((NB - NR * YN, 72, 128), BF16),
             pltpu.VMEM((NB - NR * YN, 72, 128), BF16),
             pltpu.VMEM((4, NB, 72, 128), BF16),
             pltpu.VMEM((m, 2048), BF16),
-            pltpu.VMEM((2, m, 512), BF16),
+            pltpu.VMEM((m, 1024), BF16),
             pltpu.VMEM((4, NB, 72, 128), BF16),
             pltpu.VMEM((2, NB, 72, 128), BF16),
             pltpu.VMEM((NB, 72, 128), BF16),
@@ -492,13 +509,11 @@
             pltpu.VMEM((NB, 72, 128), BF16),
             pltpu.VMEM((NB * 16, 512), BF16),
             pltpu.VMEM((NB * 8, 128), BF16),
-            pltpu.VMEM((512, 512), BF16),
-            pltpu.VMEM((256, 512), BF16),
-            dma((9,)),
+            dma((13,)),
             dma((3,)), dma((3,)),
-            dma, dma((NG,)),
-            dma, dma((2,)),
-            dma, dma((2 * NR + 2,)),
+            dma, dma((6,)),
+            dma, dma, dma((2,)),
+            dma, dma((2 * NR,)),
             dma, dma,
             dma, dma((2, 4)),
             dma, dma((NG,)),
@@ -511,7 +526,7 @@
             dma, dma,
         ],
         compiler_params=pltpu.CompilerParams(
-            collective_id=0, has_side_effects=True, vmem_limit_bytes=60 * 1024 * 1024
+            collective_id=0, has_side_effects=True, vmem_limit_bytes=64000 * 1024
         ),
     )(
         first_input, first_gain, pool_inward, pool_mixing, pool_scale, pool_outward,

time: 71.9 us -> 64.1 us (0.89); the launches traced: 71.1 us -> 64.1 us
  Pallas kernels: 66.9 us -> 61.9 us
  local copies, waits for them, and re-layouts: 3.54 us -> 1.5 us
    pallas_call x1, Pallas kernels: 66.9 us -> 61.9 us  [local(): pl.pallas_call(kernel, name='mixer_experts', out_shape=(pltpu.VMEM((512,...]
    unnamed x2, local copies, waits for them, and re-layouts: 3.54 us -> 1.5 us
where the time goes in v3:
time: 64.1 us
  Pallas kernels  61.9 us (97%)
  local copies, waits for them, and re-layouts  1.5 us (2%)
    pallas_call x1, Pallas kernels, local(): pl.pallas_call(kernel, name='mixer_experts', out_shape=(pltpu.VMEM((512,...  61.9 us
    unnamed x2, local copies, waits for them, and re-layouts  1.5 us

profile of v3, /device:TPU:1, one launch (start us, length us, event | category | flops | bytes accessed | tf_op | source)
XLA Modules:
  0.0 64.1 jit_solution(16207287792235056592)
XLA Ops:
  0.6 61.9 %mixer_experts.1 = (bf16[512,512]{1,0:T(8,128)(2,1)S(1)}, bf16[256,512]{1,0:T(8,128)(2,1)S(1)}) custom-call(bf16[512,2048]{1,0:T(8,128)(2,1)} %x1_h.1, bf16[2048]{0:T(1024)(128)(2,1)} %g1_h.1, bf16[2048,256]{1,0:T(8,128)(2,1)} %pin_h.1, bf16[1,256,256]{2,1,0:T(8,128)(2,1)} %pmix_h.1, bf16[256]{0:T(256)(128)(2,1)} %psc_h.1, bf16[256,2048]{1,0:T(8,128)(2,1)} %pout_h.1, ...), custom_call_target="tpu_custom_call" | custom-call | tf_op jit(solution)/shard_map/mixer_experts/pallas_call | solution.py:469
  62.6 0.8 %copy.17 = bf16[512,512]{1,0:T(8,128)(2,1)} copy(bf16[512,512]{1,0:T(8,128)(2,1)S(1)} %get-tuple-element.2) | data formatting | bytes 1048576
  63.4 0.7 %copy.18 = bf16[256,512]{1,0:T(8,128)(2,1)} copy(bf16[256,512]{1,0:T(8,128)(2,1)S(1)} %get-tuple-element.3) | data formatting | bytes 524288

commit v4 on v3

--- a/solution.py
+++ b/solution.py
@@ -12,7 +12,7 @@
 NB = ZN * YN
 NG = ZN
 EP = NB * 2
-HALF = NB // 2
+PAIR = 2 * YN
 ORDER = (3, 5, 4, 0, 2, 6, 1, 7)
 NR = 3
 SELF = 3 * YN
@@ -42,7 +42,7 @@
     out1, out2,
     ids, g2, g1, pmix, psc, lg, x1, pin, x2, wg, wu, wd, wg2, wu2,
     n1, pl_in, ext, halo, tail, plx, wo, xq,
-    s, s1, s2, s3, r, lhs, hid, tm, rr, rv, fin, ret, fm, fo,
+    s, s1, s2, s3, r, lhs, hid, tm, rr, rv, fin, ret, fm, acc,
     sem_in, ws_s, ws_r, a_s, a_r, a2_s, n_s, n_r, g_s, g_r, y_s, y_r, v_s, v_r, d_s, d_r,
     b_s, b_r, h_s, h_r, wo_s, wo_r, wy_s, wy_r, wp_s, wp_r, p_s, p_r, p2_s, p2_r,
 ):
@@ -227,7 +227,7 @@
 
     def pass_on(g):
         arrived(g)
-        for dx in (1, 3, 2) if g == NR - 1 else (1, 3):
+        for dx in ((1, 3), (1, 3), (1, 3, 2), (), (3,), (1,))[g]:
             gather(g, dx).start()
 
     def relay_on(g):
@@ -276,14 +276,14 @@
         whole = ORDER[g] in (0, 1, 7)
         for buf, dx, ss in ((s, 0, a_s), (s2, 2, a2_s), (s1, 1, n_s), (s3, 3, n_s)):
             if dx == 0 and g > NR:
-                send_blocks(s, 0, 0, g, a_s, n_r.at[1] if whole else a_r.at[g])
-            elif dx == 2 or (dx and whole):
-                send_blocks(buf, dx, NR * YN, g, ss, n_r.at[g // 4])
+                send_blocks(s, 0, 0, g, a_s, n_r.at[2] if whole else a_r.at[g])
+            elif dx == 2 or (dx and whole) or (g, dx) in ((4, 1), (5, 3)):
+                send_blocks(buf, dx, NR * YN, g, ss, n_r.at[0 if g == NR else 2 if whole else 1])
     pass_on(0)
     pass_on(1)
-    pass_on(2)
     relay_on(0)
     relay_on(1)
+    pass_on(2)
     pass_on(4)
     pass_on(5)
     landed(wo.at[pl.ds(1, 3), piece], wo_r)
@@ -291,18 +291,18 @@
         copy.start()
 
     def expand(k):
-        m, n = iota((HALF * 2, HALF * 8), 0), iota((HALF * 2, HALF * 8), 1)
+        m, n = iota((PAIR * 2, PAIR * 8), 0), iota((PAIR * 2, PAIR * 8), 1)
         return (n == (m // 2) * 8 + lax.rem(m, 2) * 4 + k).astype(BF16)
 
     def rows_in(i):
-        blocks = pl.ds(i * HALF, HALF)
+        blocks = pl.ds(i * PAIR, PAIR)
         for dx in range(4):
             q = quarter(-dx)
-            over = r[dx, blocks, 64:72, :].astype(F32).reshape(HALF * 8, 128).astype(BF16)
+            over = r[dx, blocks, 64:72, :].astype(F32).reshape(PAIR * 8, 128).astype(BF16)
             for k in range(4):
                 cols = pl.ds(pl.multiple_of(q * 512 + 128 * k, 128), 128)
-                lhs[0 : HALF * 16, cols] = r[dx, blocks, 16 * k : 16 * k + 16, :].reshape(HALF * 16, 128)
-                lhs[HALF * 16 : HALF * 18, cols] = dot(expand(k), over).astype(BF16)
+                lhs[0 : PAIR * 16, cols] = r[dx, blocks, 16 * k : 16 * k + 16, :].reshape(PAIR * 16, 128)
+                lhs[PAIR * 16 : PAIR * 18, cols] = dot(expand(k), over).astype(BF16)
 
     def units(n, carry):
         cols = pl.ds(n * 256, 256) if isinstance(n, int) else pl.ds(pl.multiple_of(n * 256, 256), 256)
@@ -312,19 +312,19 @@
         return carry
 
     def down(i, dx):
-        blocks = pl.ds(i * HALF, HALF)
+        blocks = pl.ds(i * PAIR, PAIR)
         cols = pl.ds(pl.multiple_of(quarter(dx) * 512, 512), 512)
         term = dot(hid[...], wd[:, cols])
-        n, m = iota((HALF * 8, HALF * 2), 0), iota((HALF * 8, HALF * 2), 1)
-        spread = dot((n // 4 == m).astype(BF16), term[HALF * 16 :].astype(BF16))
-        lane_group = lax.rem(iota((HALF * 8, 128), 0), 4)
+        n, m = iota((PAIR * 8, PAIR * 2), 0), iota((PAIR * 8, PAIR * 2), 1)
+        spread = dot((n // 4 == m).astype(BF16), term[PAIR * 16 :].astype(BF16))
+        lane_group = lax.rem(iota((PAIR * 8, 128), 0), 4)
         over = spread[:, 0:128]
         for k in range(4):
-            part = term[0 : HALF * 16, 128 * k : 128 * k + 128]
-            tm[dx, blocks, 16 * k : 16 * k + 16, :] = part.reshape(HALF, 16, 128).astype(BF16)
+            part = term[0 : PAIR * 16, 128 * k : 128 * k + 128]
+            tm[dx, blocks, 16 * k : 16 * k + 16, :] = part.reshape(PAIR, 16, 128).astype(BF16)
             if k:
                 over = jnp.where(lane_group == k, spread[:, 128 * k : 128 * k + 128], over)
-        tm[dx, blocks, 64:72, :] = over.reshape(HALF, 8, 128).astype(BF16)
+        tm[dx, blocks, 64:72, :] = over.reshape(PAIR, 8, 128).astype(BF16)
 
     def by_way(j, dx):
         rows = blocks_of(2 * j + dx // 2)
@@ -359,7 +359,7 @@
             joined(j, dx).start()
 
     def back(b):
-        return remote(fin.at[b], ret.at[b], b_s, b_r, at(ZN - group_dz(b // YN), YN - lax.rem(b, YN)))
+        return remote(fin.at[b], ret.at[b], b_s, b_r.at[b // (4 * YN)], at(ZN - group_dz(b // YN), YN - lax.rem(b, YN)))
 
     def summed(g):
         rows = blocks_of(g)
@@ -372,42 +372,51 @@
         for dy in range(YN):
             back(g * YN + dy).start()
 
-    landed(s.at[pl.ds(0, (NR - 1) * YN)], y_r)
-    landed(s.at[pl.ds(0, NR * YN)], g_r.at[2 * NR - 2])
-    landed(s.at[pl.ds(0, NR * YN)], n_r.at[0])
+    def up_part(j):
+        with jax.named_scope(f"rows{j}"):
+            rows_in(j)
+        with jax.named_scope(f"units{j}"):
+            lax.fori_loop(0, 2, units, 0)
+
+    def down_part(j):
+        with jax.named_scope(f"down{j}"):
+            down(j, 2)
+            start_by_way(j)
+            for dx in (1, 3, 0):
+                down(j, dx)
+            for dx in (1, 3):
+                direct(j, dx).start()
+
+    landed(s.at[pl.ds(0, PAIR)], y_r)
     for copy in loads[3:]:
         copy.wait()
     for copy in swaps:
         copy.wait_recv()
-    rows_in(0)
-    lax.fori_loop(0, 2, units, 0)
-    down(0, 2)
-    each(0, 2, start_by_way)
-    for dx in (1, 3):
-        down(0, dx)
-        each(0, 2, lambda j: direct(j, dx).start())
-    down(0, 0)
-    landed(s.at[pl.ds(0, HALF)], g_r.at[2 * NR - 1])
-    landed(r.at[pl.ds(0, 2), pl.ds(0, 20)], n_r.at[1])
-    rows_in(1)
-    units(0, 0)
+    up_part(0)
+    down_part(0)
+    landed(s.at[pl.ds(0, NR * YN)], g_r.at[2 * NR - 2])
+    landed(s.at[pl.ds(0, NR * YN)], n_r.at[0])
+    up_part(1)
+    down_part(1)
+    join(0)
+    landed(s.at[pl.ds(0, PAIR)], g_r.at[2 * NR - 1])
+    landed(s.at[pl.ds(0, 4 * YN)], n_r.at[1])
+    up_part(2)
+    down_part(2)
+    join(1)
     landed(wo.at[pl.ds(1, 3), pl.ds(0, 96)], wy_r)
     shared.start()
-    each(0, 2, join)
-
-    units(1, 0)
-    down(1, 2)
-    each(2, 4, start_by_way)
-    for dx in (1, 3):
-        down(1, dx)
-        each(2, 4, lambda j: direct(j, dx).start())
-    down(1, 0)
-    each(0, NR, give_back)
+    landed(s, n_r.at[2])
+    up_part(3)
+    each(0, 2, give_back)
+    down_part(3)
+    join(2)
+    give_back(2)
     summed(NR)
     ret[SELF] = fin[SELF]
     for dy in range(1, YN):
         back(SELF + dy).start()
-    each(2, 4, join)
+    join(3)
     for dx in (1, 3):
         pooled(dx).wait_recv()
         pooled_on(dx).start()
@@ -422,30 +431,41 @@
     landed(plx.at[0], p2_r)
     for n in range(2):
         rows = slice(256 * n, 256 * n + 256)
-        acc = dot(plx[0, rows, :], wo[0])
+        mixed_out = dot(plx[0, rows, :], wo[0])
         for dx in (1, 2, 3):
-            acc = acc + dot(plx[dx, rows, :], wo[dx])
-        out1[rows, :] = acc.astype(BF16)
-
-    landed(s.at[pl.ds(0, NB - 1)], b_r)
-    for k in range(4):
-        fm[:, 128 * k : 128 * k + 128] = ret[:, 16 * k : 16 * k + 16, :].reshape(NB * 16, 128)
-    fo[...] = ret[:, 64:72, :].astype(F32).reshape(NB * 8, 128).astype(BF16)
-    picks = []
-    for (main, over), share in maps:
-        base = dot((main == slot_main).astype(BF16), fm[...])
-        picks.append((base, over == slot_over, share))
-    for k in range(4):
-        acc = jnp.zeros((256, 128), F32)
-        for base, over, share in picks:
-            extra = dot(jnp.logical_and(over, over_k == k).astype(BF16), fo[...])
-            acc = acc + share * (base[:, 128 * k : 128 * k + 128] + extra)
-        out2[:, 128 * k : 128 * k + 128] = acc.astype(BF16)
+            mixed_out = mixed_out + dot(plx[dx, rows, :], wo[dx])
+        out1[rows, :] = mixed_out.astype(BF16)
+
+    def pick_up(i):
+        blocks = pl.ds(16 * i, 16)
+        for k in range(4):
+            fm[:, 128 * k : 128 * k + 128] = ret[blocks, 16 * k : 16 * k + 16, :].reshape(256, 128)
+        fo = ret[blocks, 64:72, :].astype(F32).reshape(128, 128).astype(BF16)
+        values = []
+        for (main, over), share in maps:
+            lanes = slice(256 * i, 256 * i + 256)
+            base = dot((main[:, lanes] == slot_main[:, lanes]).astype(BF16), fm[...])
+            lanes = slice(128 * i, 128 * i + 128)
+            hits = over[:, lanes] == slot_over[:, lanes]
+            marks = [jnp.logical_and(hits, over_k[:, lanes] == k).astype(BF16) for k in range(4)]
+            extra = [dot(mark, fo) for mark in marks]
+            values.append((base, extra, share))
+        return [
+            sum(share * (base[:, 128 * k : 128 * k + 128] + extra[k]) for base, extra, share in values) for k in range(4)
+        ]
+
+    landed(s.at[pl.ds(0, 15)], b_r.at[0])
+    for k, v in enumerate(pick_up(0)):
+        acc[:, 128 * k : 128 * k + 128] = v
+    landed(s.at[pl.ds(0, 16)], b_r.at[1])
+    for k, v in enumerate(pick_up(1)):
+        lanes = slice(128 * k, 128 * k + 128)
+        out2[:, lanes] = (acc[:, lanes] + v).astype(BF16)
 
     left(s.at[pl.ds(0, NB - 1)], a_s)
     left(s.at[pl.ds(0, NB - NR * YN - 1)], a2_s)
-    left(s.at[pl.ds(0, 22)], n_s)
-    left(r.at[pl.ds(0, 2), pl.ds(0, 22)], g_s)
+    left(s.at[pl.ds(0, 30)], n_s)
+    left(r.at[pl.ds(0, 2), pl.ds(0, 18)], g_s)
     left(s.at[pl.ds(0, (NR - 1) * YN)], y_s)
     left(s, v_s)
     left(r.at[pl.ds(0, 2)], d_s)
@@ -465,7 +485,7 @@
     vmem = pl.BlockSpec(memory_space=pltpu.VMEM)
     far = pl.BlockSpec(memory_space=pl.ANY)
     dma = pltpu.SemaphoreType.DMA
-    m = HALF * 18
+    m = PAIR * 18
     return pl.pallas_call(
         kernel,
         name="mixer_experts",
@@ -507,17 +527,17 @@
             pltpu.VMEM((NB, 72, 128), BF16),
             pltpu.VMEM((NB, 72, 128), BF16),
             pltpu.VMEM((NB, 72, 128), BF16),
-            pltpu.VMEM((NB * 16, 512), BF16),
-            pltpu.VMEM((NB * 8, 128), BF16),
+            pltpu.VMEM((256, 512), BF16),
+            pltpu.VMEM((256, 512), F32),
             dma((13,)),
             dma((3,)), dma((3,)),
             dma, dma((6,)),
-            dma, dma, dma((2,)),
+            dma, dma, dma((3,)),
             dma, dma((2 * NR,)),
             dma, dma,
             dma, dma((2, 4)),
             dma, dma((NG,)),
-            dma, dma,
+            dma, dma((2,)),
             dma, dma,
             dma, dma,
             dma, dma,

time: 64.1 us -> 62.5 us (0.975); the launches traced: 64.1 us -> 61.6 us
  Pallas kernels: 61.9 us -> 59.5 us
    pallas_call x1, Pallas kernels: 61.9 us -> 59.5 us  [local(): pl.pallas_call(kernel, name='mixer_experts', out_shape=(pltpu.VMEM((512,...]
where the time goes in v4:
time: 62.5 us; the launch traced here: 61.6 us
  Pallas kernels  59.5 us (95%)
  local copies, waits for them, and re-layouts  1.5 us (2%)
  between operations  0.64 us (1%)
    pallas_call x1, Pallas kernels, local(): pl.pallas_call(kernel, name='mixer_experts', out_shape=(pltpu.VMEM((512,...  59.5 us
    unnamed x2, local copies, waits for them, and re-layouts  1.5 us

profile of v4, /device:TPU:1, one launch (start us, length us, event | category | flops | bytes accessed | tf_op | source)
XLA Modules:
  0.0 61.6 jit_solution(16985864534913224578)
XLA Ops:
  0.6 59.5 %mixer_experts.1 = (bf16[512,512]{1,0:T(8,128)(2,1)S(1)}, bf16[256,512]{1,0:T(8,128)(2,1)S(1)}) custom-call(bf16[512,2048]{1,0:T(8,128)(2,1)} %x1_h.1, bf16[2048]{0:T(1024)(128)(2,1)} %g1_h.1, bf16[2048,256]{1,0:T(8,128)(2,1)} %pin_h.1, bf16[1,256,256]{2,1,0:T(8,128)(2,1)} %pmix_h.1, bf16[256]{0:T(256)(128)(2,1)} %psc_h.1, bf16[256,2048]{1,0:T(8,128)(2,1)} %pout_h.1, ...), custom_call_target="tpu_custom_call" | custom-call | tf_op jit(solution)/shard_map/mixer_experts/pallas_call | solution.py:489
  60.1 0.8 %copy.17 = bf16[512,512]{1,0:T(8,128)(2,1)} copy(bf16[512,512]{1,0:T(8,128)(2,1)S(1)} %get-tuple-element.2) | data formatting | bytes 1048576
  60.9 0.7 %copy.18 = bf16[256,512]{1,0:T(8,128)(2,1)} copy(bf16[256,512]{1,0:T(8,128)(2,1)S(1)} %get-tuple-element.3) | data formatting | bytes 524288

commit v5 on v4

--- a/solution.py
+++ b/solution.py
@@ -52,14 +52,14 @@
     y, z = lax.rem(chip, YN), chip // YN
 
     def at(dz, dy, dc=0):
-        z2, y2, c2 = lax.rem(z + dz + ZN, ZN), lax.rem(y + dy + YN, YN), lax.rem(c + dc, 2)
+        z2, y2, c2 = (z + dz + ZN) & (ZN - 1), (y + dy + YN) & (YN - 1), (c + dc) & 1
         return ((z2 * YN + y2) * 2 + c2, t)
 
     def along(dx):
-        return (ep, lax.rem(t + dx, XN))
+        return (ep, (t + dx) & (XN - 1))
 
     def quarter(dx):
-        return lax.rem(t + dx + XN, XN)
+        return (t + dx + XN) & (XN - 1)
 
     partner = at(0, 0, 1)
     following = (lax.rem(ep + 1, EP), t)
@@ -88,12 +88,9 @@
 
     bar = pltpu.get_barrier_semaphore()
 
-    def greet(b, carry):
-        pl.semaphore_signal(bar, inc=1, device_id=at(group_dz(b // YN), lax.rem(b, YN)), device_id_type=MESH)
-        return carry
-
-    lax.fori_loop(0, SELF, greet, 0)
-    lax.fori_loop(SELF + 1, NB, greet, 0)
+    for b in range(NB):
+        if b != SELF:
+            pl.semaphore_signal(bar, inc=1, device_id=at(ORDER[b // YN], b % YN), device_id_type=MESH)
     for dx in (1, 2, 3):
         pl.semaphore_signal(bar, inc=1, device_id=along(dx), device_id_type=MESH)
     pl.semaphore_signal(bar, inc=1, device_id=partner, device_id_type=MESH)

time: 62.5 us -> 61.8 us (0.989); the launches traced: 61.6 us -> 61.6 us
  no operation moved by 1% of the time
where the time goes in v5:
time: 61.8 us; the launch traced here: 61.6 us
  Pallas kernels  59.5 us (96%)
  local copies, waits for them, and re-layouts  1.5 us (2%)
  between operations  0.64 us (1%)
    pallas_call x1, Pallas kernels, local(): pl.pallas_call(kernel, name='mixer_experts', out_shape=(pltpu.VMEM((512,...  59.5 us
    unnamed x2, local copies, waits for them, and re-layouts  1.5 us

profile of v5, /device:TPU:1, one launch (start us, length us, event | category | flops | bytes accessed | tf_op | source)
XLA Modules:
  0.0 61.6 jit_solution(1166380617602769649)
XLA Ops:
  0.6 59.5 %mixer_experts.1 = (bf16[512,512]{1,0:T(8,128)(2,1)S(1)}, bf16[256,512]{1,0:T(8,128)(2,1)S(1)}) custom-call(bf16[512,2048]{1,0:T(8,128)(2,1)} %x1_h.1, bf16[2048]{0:T(1024)(128)(2,1)} %g1_h.1, bf16[2048,256]{1,0:T(8,128)(2,1)} %pin_h.1, bf16[1,256,256]{2,1,0:T(8,128)(2,1)} %pmix_h.1, bf16[256]{0:T(256)(128)(2,1)} %psc_h.1, bf16[256,2048]{1,0:T(8,128)(2,1)} %pout_h.1, ...), custom_call_target="tpu_custom_call" | custom-call | tf_op jit(solution)/shard_map/mixer_experts/pallas_call | solution.py:486
  60.1 0.8 %copy.17 = bf16[512,512]{1,0:T(8,128)(2,1)} copy(bf16[512,512]{1,0:T(8,128)(2,1)S(1)} %get-tuple-element.2) | data formatting | bytes 1048576
  60.9 0.7 %copy.18 = bf16[256,512]{1,0:T(8,128)(2,1)} copy(bf16[256,512]{1,0:T(8,128)(2,1)S(1)} %get-tuple-element.3) | data formatting | bytes 524288

commit v6 on v5

--- a/solution.py
+++ b/solution.py
@@ -83,7 +83,7 @@
         pltpu.make_async_copy(a, b, sem_in.at[7 + i])
         for i, (a, b) in enumerate([(ids_h, ids), (g2_h, g2), (g1_h, g1), (pmix_h, pmix), (psc_h, psc), (lg_h, lg)])
     ]
-    for copy in small + loads:
+    for copy in small[:2] + loads[:1] + small[2:3] + loads[1:3] + small[3:]:
         copy.start()
 
     bar = pltpu.get_barrier_semaphore()
@@ -96,8 +96,7 @@
     pl.semaphore_signal(bar, inc=1, device_id=partner, device_id_type=MESH)
     pl.semaphore_signal(bar, inc=1, device_id=previous, device_id_type=MESH)
 
-    for copy in small:
-        copy.wait()
+    small[0].wait()
     expert = iota((NB, 256), 0)
     one0 = (ids[0:1, :] == expert).astype(F32)
     one1 = (ids[1:2, :] == expert).astype(F32)
@@ -120,6 +119,7 @@
     slot_over = (lax.rem(over_col // 4, 2) + 17).astype(F32)
     over_k = lax.rem(over_col, 4)
 
+    small[1].wait()
     loads[0].wait()
 
     def norm2(i, carry):
@@ -150,6 +150,7 @@
 
     fill(s, 0, 0)
 
+    small[2].wait()
     loads[1].wait()
     loads[2].wait()
 
@@ -196,7 +197,7 @@
         remote(a, b, ws_s.at[i], ws_r.at[i], partner)
         for i, (a, b) in enumerate([(wg_h.at[0], wg2), (wu_h.at[0], wu2), (wd_h.at[0], wd.at[pl.ds(512, 512)])])
     ]
-    for copy in swaps:
+    for copy in swaps + loads[3:]:
         copy.start()
 
     own_out = pltpu.make_async_copy(
@@ -245,6 +246,8 @@
 
     lax.fori_loop(0, 2, inward, 0)
 
+    for copy in small[3:]:
+        copy.wait()
     halo_copy.wait_recv()
     ext[0:16, :] = jnp.where(ep == 0, 0.0, halo[...].astype(F32))
     ext[16:528, :] = pl_in[...].astype(F32)

time: 61.8 us -> 63 us (1.019)
  Pallas kernels: 59.5 us -> 60.8 us
    pallas_call x1, Pallas kernels: 59.5 us -> 60.8 us  [local(): pl.pallas_call(kernel, name='mixer_experts', out_shape=(pltpu.VMEM((512,...]
where the time goes in v6:
time: 63 us; the launch traced here: 62.9 us
  Pallas kernels  60.8 us (97%)
  local copies, waits for them, and re-layouts  1.5 us (2%)
  between operations  0.64 us (1%)
    pallas_call x1, Pallas kernels, local(): pl.pallas_call(kernel, name='mixer_experts', out_shape=(pltpu.VMEM((512,...  60.8 us
    unnamed x2, local copies, waits for them, and re-layouts  1.5 us

profile of v6, /device:TPU:1, one launch (start us, length us, event | category | flops | bytes accessed | tf_op | source)
XLA Modules:
  0.0 62.9 jit_solution(16518775836565231280)
XLA Ops:
  0.6 60.8 %mixer_experts.1 = (bf16[512,512]{1,0:T(8,128)(2,1)S(1)}, bf16[256,512]{1,0:T(8,128)(2,1)S(1)}) custom-call(bf16[512,2048]{1,0:T(8,128)(2,1)} %x1_h.1, bf16[2048]{0:T(1024)(128)(2,1)} %g1_h.1, bf16[2048,256]{1,0:T(8,128)(2,1)} %pin_h.1, bf16[1,256,256]{2,1,0:T(8,128)(2,1)} %pmix_h.1, bf16[256]{0:T(256)(128)(2,1)} %psc_h.1, bf16[256,2048]{1,0:T(8,128)(2,1)} %pout_h.1, ...), custom_call_target="tpu_custom_call" | custom-call | tf_op jit(solution)/shard_map/mixer_experts/pallas_call | solution.py:489
  61.4 0.8 %copy.17 = bf16[512,512]{1,0:T(8,128)(2,1)} copy(bf16[512,512]{1,0:T(8,128)(2,1)S(1)} %get-tuple-element.2) | data formatting | bytes 1048576
  62.2 0.7 %copy.18 = bf16[256,512]{1,0:T(8,128)(2,1)} copy(bf16[256,512]{1,0:T(8,128)(2,1)S(1)} %get-tuple-element.3) | data formatting | bytes 524288
